TPU v7x, 32 devices: a whole 2x2x4 slice. The times are simulated.
32 devices in a mesh: ep: 16 (over z, y, x), tp: 2 (over core).
Axes of the slice: x: 2, y: 2, z: 4, core: 2. Of those that a mesh axis runs over, the one named last changes fastest.
Arguments:
- hidden: bfloat16 [1024, 2048], P('ep'), may hold values from -6 to 6
- mix_gain: float32 [2048], replicated, may hold values from 0.1 to 1.9
- recept_weight: bfloat16 [2048, 1024], P(None, 'tp'), may hold values from -0.125 to 0.125
- key_weight: bfloat16 [2048, 1024], P(None, 'tp'), may hold values from -0.125 to 0.125
- value_weight: bfloat16 [2048, 1024], P(None, 'tp'), may hold values from -0.125 to 0.125
- decay_down: bfloat16 [2048, 64], replicated, may hold values from -0.125 to 0.125
- decay_up: bfloat16 [64, 1024], replicated, may hold values from -0.75 to 0.75
- decay_bias: float32 [1024], replicated, may hold values from -4 to 1
- rate_down: bfloat16 [2048, 64], replicated, may hold values from -0.125 to 0.125
- rate_up: bfloat16 [64, 1024], replicated, may hold values from -0.75 to 0.75
- rate_bias: float32 [1024], replicated, may hold values from -4 to 4
- head_gain: float32 [1024], replicated, may hold values from 0.1 to 1.9
- out_weight: bfloat16 [1024, 2048], P('tp'), may hold values from -0.1875 to 0.1875
- memory_state: float32 [1024, 16, 64, 64], P('ep', 'tp'), may hold values from -6 to 6
- ffn_gain: float32 [2048], replicated, may hold values from 0.1 to 1.9
- blend_vector: bfloat16 [2048], replicated, may hold values from -0.125 to 0.125
- dense_gate: bfloat16 [2048, 5632], P(None, ('ep', 'tp')), may hold values from -0.125 to 0.125
- dense_up: bfloat16 [2048, 5632], P(None, ('ep', 'tp')), may hold values from -0.125 to 0.125
- dense_down: bfloat16 [5632, 2048], P(('ep', 'tp')), may hold values from -0.3125 to 0.3125
- expert_gate: bfloat16 [16, 2048, 1536], P('ep', None, 'tp'), may hold values from -0.125 to 0.125
- expert_up: bfloat16 [16, 2048, 1536], P('ep', None, 'tp'), may hold values from -0.125 to 0.125
- expert_down: bfloat16 [16, 1536, 2048], P('ep', 'tp'), may hold values from -0.15625 to 0.15625
- routing: int32 [1024, 2], P('ep'), may hold values from 0 to 15, all different within a row; in each aligned block of 64 rows (0 to 63, 64 to 127, ...) at most 16 rows name the same one
- route_scale: float32 [1024, 2], P('ep'), may hold values from 0.25 to 1
Outputs:
- layer_out: bfloat16 [1024, 2048], P('ep')
- new_state: float32 [1024, 16, 64, 64], P('ep', 'tp')
Inputs may be any that keep to these rules, and one draw needn't show every extreme that they name: `routing`: among the 64 sequences of one index of ep, no expert is chosen more than 16 times, and some expert is chosen exactly 16 times; a sequence's 2 choices differ.
All inputs are finite; a program needn't handle non-finite values.
Results may differ from a plain program's by a relative error of at most 0.017.
Values may be sent and summed in bfloat16 or wider, within the bound.
A program may use at most 192 MiB of HBM per device.

v0:
```python
import functools
import math

import jax
import jax.numpy as jnp
from jax import lax
from jax.experimental import pallas as pl
from jax.experimental.pallas import tpu as pltpu
from jax.sharding import PartitionSpec as P

MESH = pl.DeviceIdType.MESH
F32 = jnp.float32
BF16 = jnp.bfloat16
VMEM_LIMIT = 64 * 1024 * 1024 - 65536
VMEM_SPEC = pl.BlockSpec(memory_space=pltpu.VMEM)


def matmul(left, right):
    return jnp.dot(left, right, preferred_element_type=F32)


def matmul_nt(left, right):
    return lax.dot_general(left, right, (((1,), (1,)), ((), ())), preferred_element_type=F32)


def silu_of(tensor):
    return tensor / (1.0 + jnp.exp(-tensor))


def rms_scaled(values, gain):
    return values * lax.rsqrt(jnp.mean(values * values, axis=-1, keepdims=True) + 1e-06) * gain


def factors_of(count):
    slow = 4 if count % 4 == 0 else 1
    rest = count // slow
    mid = math.isqrt(rest)
    while rest % mid:
        mid -= 1
    return slow, mid, rest // mid


def attention_kernel(
    step_rows,
    hidden,
    mix_gain,
    recept_weight,
    key_weight,
    value_weight,
    decay_down,
    decay_up,
    decay_bias,
    rate_down,
    rate_up,
    rate_bias,
    head_gain,
    out_weight,
    state_in,
    state_out,
    partial,
    recept_s,
    unit_s,
    unit_rate_s,
    key_rate_s,
    value_s,
    decay_s,
    readout_s,
    normed_s,
):
    step = pl.program_id(0)
    heads, seqs, size = recept_s.shape
    width = heads * size
    own = pl.ds(pl.multiple_of(lax.axis_index("tp") * width, 128), width)

    @pl.when(step == 0)
    def _():
        normed = rms_scaled(hidden[...].astype(F32), mix_gain[...]).astype(BF16)
        recept = matmul(normed, recept_weight[...]).astype(BF16).astype(F32)
        keys = matmul(normed, key_weight[...]).astype(BF16).astype(F32)
        vals = matmul(normed, value_weight[...]).astype(BF16).astype(F32)
        decay_low = jnp.tanh(matmul_nt(normed, decay_down[...])).astype(BF16)
        decay_pre = matmul(decay_low, decay_up[:, own]) + decay_bias[:, own]
        softplus = jnp.maximum(-decay_pre, 0.0) + jnp.log1p(jnp.exp(-jnp.abs(decay_pre)))
        decay = jnp.exp(-jnp.exp(-softplus - 0.5))
        rate_low = matmul_nt(normed, rate_down[...]).astype(BF16)
        rate = 1.0 / (1.0 + jnp.exp(-(matmul(rate_low, rate_up[:, own]) + rate_bias[:, own])))
        for h in range(heads):
            cols = slice(h * size, (h + 1) * size)
            key_h, rate_h = keys[:, cols], rate[:, cols]
            unit = key_h * lax.rsqrt(jnp.sum(key_h * key_h, axis=-1, keepdims=True) + 1e-06)
            recept_s[h] = recept[:, cols]
            unit_s[h] = unit
            unit_rate_s[h] = unit * rate_h
            key_rate_s[h] = key_h * rate_h
            value_s[h] = vals[:, cols]
            decay_s[h] = decay[:, cols]

    shape, flat = (heads, size, size), (heads * size, size)
    eye = lax.broadcasted_iota(jnp.int32, shape, 1) == lax.broadcasted_iota(jnp.int32, shape, 2)
    ones = jnp.ones((size, size), BF16)

    def row_sums(values):
        return matmul(values.astype(BF16).reshape(flat), ones).reshape(shape)

    def one_sequence(local, carry):
        row = pl.ds(step * step_rows + local, 1)
        state = state_in[local]
        removed = row_sums(state * unit_s[:, row])
        value = row_sums(jnp.where(eye, value_s[:, row], 0.0))
        new = (
            state * decay_s[:, row] - removed * unit_rate_s[:, row] + value * key_rate_s[:, row]
        )
        state_out[local] = new
        out = row_sums(new * recept_s[:, row])
        readout_s[:, row] = jnp.sum(jnp.where(eye, out, 0.0), axis=1, keepdims=True)
        return carry

    lax.fori_loop(0, step_rows, one_sequence, 0, unroll=4)

    @pl.when(step == pl.num_programs(0) - 1)
    def _():
        gain = head_gain[:, own]
        for h in range(heads):
            cols = slice(h * size, (h + 1) * size)
            out = readout_s[h]
            centred = out - jnp.mean(out, axis=-1, keepdims=True)
            variance = jnp.mean(centred * centred, axis=-1, keepdims=True)
            normed_s[:, cols] = (centred * lax.rsqrt(variance + 0.00064) * gain[:, cols]).astype(BF16)
        partial[...] = matmul(normed_s[...], out_weight[...]).astype(BF16)


def attention(hidden, vectors, state):
    seqs, heads, size, _ = state.shape
    width = heads * size
    step_rows = math.gcd(seqs, 8)
    block = pl.BlockSpec((step_rows, heads, size, size), lambda i: (i, 0, 0, 0))
    operands = (hidden,) + vectors
    whole = [pl.BlockSpec(a.shape, lambda i: (0, 0)) for a in operands]
    per_head = pltpu.VMEM((heads, seqs, size), F32)
    return pl.pallas_call(
        functools.partial(attention_kernel, step_rows),
        grid=(seqs // step_rows,),
        out_shape=(
            jax.ShapeDtypeStruct(state.shape, F32),
            jax.ShapeDtypeStruct(hidden.shape, BF16),
        ),
        in_specs=whole + [block],
        out_specs=(block, pl.BlockSpec(hidden.shape, lambda i: (0, 0))),
        scratch_shapes=[per_head] * 7 + [pltpu.VMEM((seqs, width), BF16)],
        compiler_params=pltpu.CompilerParams(
            dimension_semantics=("arbitrary",), vmem_limit_bytes=VMEM_LIMIT
        ),
        name="attention",
    )(*operands, state)


def position(sizes):
    ep = lax.axis_index("ep")
    strides = (sizes[1] * sizes[2], sizes[2], 1)
    return ep, tuple(ep // s % n for s, n in zip(strides, sizes)), strides


def greet_all(count):
    ep, tp = lax.axis_index("ep"), lax.axis_index("tp")
    barrier = pltpu.get_barrier_semaphore()

    def greet(k, carry):
        pl.semaphore_signal(
            barrier, inc=1, device_id=((ep + k) % count, tp), device_id_type=MESH
        )
        return carry

    lax.fori_loop(1, count, greet, 0)
    pl.semaphore_signal(barrier, inc=1, device_id=(ep, 1 - tp), device_id_type=MESH)
    pl.semaphore_wait(barrier, count)


def remote(src, dst, send, recv, device):
    return pltpu.make_async_remote_copy(
        src_ref=src,
        dst_ref=dst,
        send_sem=send,
        recv_sem=recv,
        device_id=device,
        device_id_type=MESH,
    )


def gather_kernel(
    sizes,
    partial,
    hidden,
    gain,
    meta,
    first,
    tokens,
    metas,
    sibling_part,
    part_sem,
    meta_send,
    meta_recv,
    send_sem,
    recv_sem,
    pass_send,
    pass_recv,
):
    count = sizes[0] * sizes[1] * sizes[2]
    ep, at, strides = position(sizes)
    tp = lax.axis_index("tp")
    half = first.shape[0]
    mine = pl.ds(pl.multiple_of(tp * half, half), half)
    other = pl.ds(pl.multiple_of((1 - tp) * half, half), half)
    greet_all(count)
    swap = remote(partial.at[other], sibling_part, part_sem.at[0], part_sem.at[1], (ep, 1 - tp))
    swap.start()

    def meta_copy(k):
        return remote(
            meta, metas.at[ep], meta_send.at[k], meta_recv.at[k], ((ep + k) % count, tp)
        )

    def start_meta(k, carry):
        meta_copy(k).start()
        return carry

    lax.fori_loop(1, count, start_meta, 0)
    metas[ep] = meta[...]
    swap.wait()
    total = (
        hidden[mine, :].astype(F32)
        + partial[mine, :].astype(F32)
        + sibling_part[...].astype(F32)
    ).astype(BF16)
    first[...] = total
    ffn_in = rms_scaled(total.astype(F32), gain[...]).astype(BF16)
    tokens[at[0], at[1], at[2], mine, :] = ffn_in

    def views(order, r):
        _, d2, d3 = order

        def view(k, second, third):
            spot = [pl.ds((at[0] + sizes[0] - k) % sizes[0], 1), None, None]
            spot[d2], spot[d3] = second, third
            return tokens.at[tuple(spot) + (r,)]

        def one(d, j=0):
            return pl.ds((at[d] + sizes[d] - j) % sizes[d], 1)

        whole = pl.ds(0, sizes[d2])
        return (
            lambda k, j=0: view(k, one(d2), one(d3)),
            lambda k, j=0: view(k, one(d2, j), one(d3)),
            lambda k, j=0: view(k, whole, one(d3, j)),
        )

    def run(core, order, order_of_other):
        sibling = (ep, 1 - core)
        come = views(order, pl.ds(core * half, half))
        chunks = sizes[0]
        flights, passed = {}, []

        def send(stage, k, j):
            d = order[stage]
            source = come[stage](0 if stage == 0 else k)
            peer = ep + ((at[d] + j) % sizes[d] - at[d]) * strides[d]
            slot = (stage, k, j if stage else 0)
            copy = remote(source, source, send_sem.at[slot], recv_sem.at[slot], (peer, core))
            copy.start()
            flights[slot] = copy

        def onward(stage, k, j):
            view = come[stage](k, j)
            slot = (stage, k, j)
            copy = remote(view, view, pass_send.at[slot], pass_recv.at[slot], sibling)
            copy.start()
            passed.append(copy)

        def first_phase(k):
            if k:
                flights[0, k, 0].wait()
            for j in range(1, sizes[order[1]]):
                send(1, k, j)
            onward(0, k, 0)

        def later_phase(stage, k):
            for j in range(1, sizes[order[stage]]):
                flights[stage, k, j].wait()
            if stage == 1:
                for j in range(1, sizes[order[2]]):
                    send(2, k, j)
            for j in range(1, sizes[order[stage]]):
                onward(stage, k, j)

        first_phase(0)
        for k in range(1, chunks):
            send(0, k, k)
        for t in range(chunks + 2):
            if 0 <= t - 1 < chunks:
                later_phase(1, t - 1)
            if 0 < t < chunks:
                first_phase(t)
            if 0 <= t - 2 < chunks:
                later_phase(2, t - 2)
        for copy in passed:
            copy.wait_send()
        theirs = views(order_of_other, pl.ds((1 - core) * half, half))
        for stage in range(3):
            for k in range(chunks):
                for j in range(1, sizes[order_of_other[stage]]) if stage else (0,):
                    view, slot = theirs[stage](k, j), (stage, k, j)
                    remote(view, view, pass_send.at[slot], pass_recv.at[slot], sibling).wait_recv()

    @pl.when(tp == 0)
    def _():
        run(0, (0, 2, 1), (0, 1, 2))

    @pl.when(tp == 1)
    def _():
        run(1, (0, 1, 2), (0, 2, 1))

    def wait_meta(k, carry):
        meta_copy(k).wait()
        return carry

    lax.fori_loop(1, count, wait_meta, 0)


def gather_tokens(sizes, partial, hidden, gain, meta):
    seqs, width = hidden.shape
    count = sizes[0] * sizes[1] * sizes[2]
    half = seqs // 2
    most = max(sizes)
    dma = pltpu.SemaphoreType.DMA
    return pl.pallas_call(
        functools.partial(gather_kernel, sizes),
        out_shape=(
            jax.ShapeDtypeStruct((half, width), BF16),
            jax.ShapeDtypeStruct(sizes + (seqs, width), BF16),
            jax.ShapeDtypeStruct((count,) + meta.shape, F32),
        ),
        in_specs=[VMEM_SPEC] * 4,
        out_specs=(VMEM_SPEC,) * 3,
        scratch_shapes=[
            pltpu.VMEM((half, width), BF16),
            dma((2,)),
            dma((count,)),
            dma((count,)),
            dma((3, sizes[0], most)),
            dma((3, sizes[0], most)),
            dma((3, sizes[0], most)),
            dma((3, sizes[0], most)),
        ],
        compiler_params=pltpu.CompilerParams(
            collective_id=0, has_side_effects=True, vmem_limit_bytes=VMEM_LIMIT
        ),
        name="gather_tokens",
    )(partial, hidden, gain, meta)


def scatter_kernel(sizes, parts, first, out, total, from_sibling, land0, land1, sems):
    pair_send, pair_recv, send_sem, recv_sem, last_sem = sems
    ep, at, strides = position(sizes)
    tp = lax.axis_index("tp")
    half = first.shape[0]
    mine = pl.ds(pl.multiple_of(tp * half, half), half)
    other = pl.ds(pl.multiple_of((1 - tp) * half, half), half)
    chunks = sizes[0]
    goals = [(at[0] + 1 + k) % chunks for k in range(chunks)]
    greet_all(sizes[0] * sizes[1] * sizes[2])
    pairs = []
    for k in range(chunks):
        copy = remote(
            parts.at[goals[k], :, :, other],
            from_sibling.at[k],
            pair_send.at[k],
            pair_recv.at[k],
            (ep, 1 - tp),
        )
        copy.start()
        pairs.append(copy)

    def run(core, d1, d2, lands):
        rows = pl.ds(core * half, half)
        flights = {}

        def spot(k, c1, c2):
            place = [goals[k], None, None]
            place[d1], place[d2] = c1, c2
            return tuple(place)

        def send(stage, k, j, source, dst, d):
            peer = ep + ((at[d] + j) % sizes[d] - at[d]) * strides[d]
            slot = (stage, k, j if stage < 2 else 0)
            copy = remote(source, dst, send_sem.at[slot], recv_sem.at[slot], (peer, core))
            copy.start()
            flights[slot] = copy

        def pair_sum(k):
            pairs[k].wait()

            def add(b, carry):
                y, x = b // sizes[2], b % sizes[2]
                total[goals[k], y, x] = (
                    parts[goals[k], y, x, rows, :].astype(F32) + from_sibling[k, y, x].astype(F32)
                ).astype(BF16)
                return carry

            lax.fori_loop(0, sizes[1] * sizes[2], add, 0)
            for j in range(1, sizes[d1]):
                source = total.at[spot(k, (at[d1] + j) % sizes[d1], slice(None))]
                send(0, k, j, source, lands[0].at[k, j - 1], d1)

        def first_sum(k):
            for j in range(1, sizes[d1]):
                flights[0, k, j].wait()

            def add(b, carry):
                place = spot(k, at[d1], b)
                value = total[place].astype(F32)
                for j in range(1, sizes[d1]):
                    value = value + lands[0][k, j - 1, b].astype(F32)
                total[place] = value.astype(BF16)
                return carry

            lax.fori_loop(0, sizes[d2], add, 0)
            for j in range(1, sizes[d2]):
                source = total.at[spot(k, at[d1], (at[d2] + j) % sizes[d2])]
                send(1, k, j, source, lands[1].at[k, j - 1], d2)

        def second_sum(k):
            for j in range(1, sizes[d2]):
                flights[1, k, j].wait()
            place = spot(k, at[d1], at[d2])
            value = total[place].astype(F32)
            for j in range(1, sizes[d2]):
                value = value + lands[1][k, j - 1].astype(F32)
            if k < chunks - 1:
                total[place] = value.astype(BF16)
                send(2, k, k + 1, total.at[place], lands[2].at[k], 0)
                return
            value = value + first[...].astype(F32)
            for i in range(chunks - 1):
                flights[2, i, 0].wait()
                value = value + lands[2][i].astype(F32)
            out[rows, :] = value.astype(BF16)

        for t in range(chunks + 2):
            if t < chunks:
                pair_sum(t)
            if 0 <= t - 1 < chunks:
                first_sum(t - 1)
            if 0 <= t - 2 < chunks:
                second_sum(t - 2)

    @pl.when(tp == 0)
    def _():
        run(0, 1, 2, land0)

    @pl.when(tp == 1)
    def _():
        run(1, 2, 1, land1)

    swap = remote(out.at[mine], out.at[mine], last_sem.at[0], last_sem.at[1], (ep, 1 - tp))
    swap.start()
    swap.wait()


def landing(sizes, d1, d2, half, width):
    chunks, block = sizes[0], (half, width)
    return [
        pltpu.VMEM((chunks, max(1, sizes[d1] - 1), sizes[d2]) + block, BF16),
        pltpu.VMEM((chunks, max(1, sizes[d2] - 1)) + block, BF16),
        pltpu.VMEM((max(1, chunks - 1),) + block, BF16),
    ]


def scatter_sum(sizes, parts, first):
    half, width = first.shape
    most = max(sizes)
    dma = pltpu.SemaphoreType.DMA
    return pl.pallas_call(
        functools.partial(scatter_kernel, sizes),
        out_shape=jax.ShapeDtypeStruct((2 * half, width), BF16),
        in_specs=[VMEM_SPEC] * 2,
        out_specs=VMEM_SPEC,
        scratch_shapes=[
            pltpu.VMEM(sizes + (half, width), BF16),
            pltpu.VMEM(sizes + (half, width), BF16),
            landing(sizes, 1, 2, half, width),
            landing(sizes, 2, 1, half, width),
            [
                dma((sizes[0],)),
                dma((sizes[0],)),
                dma((3, sizes[0], most)),
                dma((3, sizes[0], most)),
                dma((2,)),
            ],
        ],
        compiler_params=pltpu.CompilerParams(
            collective_id=1, has_side_effects=True, vmem_limit_bytes=VMEM_LIMIT
        ),
        name="scatter_sum",
    )(parts, first)


def shards(
    hidden,
    mix_gain,
    recept_weight,
    key_weight,
    value_weight,
    decay_down,
    decay_up,
    decay_bias,
    rate_down,
    rate_up,
    rate_bias,
    head_gain,
    out_weight,
    memory_state,
    ffn_gain,
    blend_vector,
    dense_gate,
    dense_up,
    dense_down,
    expert_gate,
    expert_up,
    expert_down,
    routing,
    route_scale,
):
    seqs, width = hidden.shape
    count = lax.axis_size("ep")
    sizes = factors_of(count)
    top = routing.shape[1]
    cap = max(2, 2 * seqs * top // count)
    new_state, partial = attention(
        hidden,
        (
            mix_gain[None],
            recept_weight,
            key_weight,
            value_weight,
            decay_down.T,
            decay_up,
            decay_bias[None],
            rate_down.T,
            rate_up,
            rate_bias[None],
            head_gain[None],
            out_weight,
        ),
        memory_state,
    )
    meta = jnp.concatenate([routing.T.astype(F32), route_scale.T], axis=0)
    meta = jnp.pad(meta, ((0, -2 * top % 8), (0, -seqs % 128)))
    first, tokens, metas = gather_tokens(sizes, partial, hidden, ffn_gain[None], meta)
    tokens = tokens.reshape(count * seqs, width)

    hit = metas[:, :top, :seqs] == lax.axis_index("ep").astype(F32)
    chosen = jnp.any(hit, axis=1)
    scale_of = jnp.sum(jnp.where(hit, metas[:, top : 2 * top, :seqs], 0.0), axis=1)
    earlier = jnp.arange(seqs)[:, None] < jnp.arange(seqs)[None, :]
    rank = matmul(chosen.astype(BF16), earlier.astype(BF16)).astype(jnp.int32)
    place = jnp.where(chosen, rank + jnp.arange(count, dtype=jnp.int32)[:, None] * cap, -1)
    select = place.reshape(1, -1) == jnp.arange(count * cap, dtype=jnp.int32)[:, None]
    slot_scale = jnp.sum(jnp.where(select, scale_of.reshape(1, -1), 0.0), axis=1, keepdims=True)
    picked = matmul(select.astype(BF16), tokens).astype(BF16)
    expert_act = (silu_of(matmul(picked, expert_gate[0])) * matmul(picked, expert_up[0])).astype(BF16)
    expert_out = (matmul(expert_act, expert_down[0]) * slot_scale).astype(BF16)
    blend = jax.nn.sigmoid(matmul_nt(tokens, blend_vector[None]))
    dense_act = (
        silu_of(matmul(tokens, dense_gate)) * matmul(tokens, dense_up) * blend
    ).astype(BF16)
    spread = (place.reshape(-1, 1) == jnp.arange(count * cap, dtype=jnp.int32)[None, :]).astype(BF16)
    parts = matmul(
        jnp.concatenate([spread, dense_act], axis=1),
        jnp.concatenate([expert_out, dense_down], axis=0),
    ).astype(BF16)
    layer_out = scatter_sum(sizes, parts.reshape(sizes + (seqs, width)), first)
    return (layer_out, new_state)


def solution(mesh):
    in_specs = (
        P("ep", None),
        P(),
        P(None, "tp"),
        P(None, "tp"),
        P(None, "tp"),
        P(),
        P(),
        P(),
        P(),
        P(),
        P(),
        P(),
        P("tp", None),
        P("ep", "tp", None, None),
        P(),
        P(),
        P(None, ("ep", "tp")),
        P(None, ("ep", "tp")),
        P(("ep", "tp"), None),
        P("ep", None, "tp"),
        P("ep", None, "tp"),
        P("ep", "tp", None),
        P("ep", None),
        P("ep", None),
    )
    out_specs = (P("ep", None), P("ep", "tp", None, None))
    return jax.shard_map(shards, mesh=mesh, in_specs=in_specs, out_specs=out_specs, check_vma=False)
```

profile of v0, /device:TPU:0, one launch (start us, length us, event | category | flops | bytes accessed | tf_op | source)
XLA Modules:
  0.0 133.8 jit_solution(7443754944604411382)
XLA Ops:
  0.6 0.5 iota_multiply_fusion
  1.2 0.7 convert_bitcast_fusion
  1.9 1.3 select_maximum_fusion.meta
  3.1 1.3 reshape.32
  4.4 25.7 %attention.1 = (f32[64,8,64,64]{3,2,1,0:T(8,128)}, bf16[64,2048]{1,0:T(8,128)(2,1)}) custom-call(bf16[64,2048]{1,0:T(8,128)(2,1)} %hidden.3, f32[1,2048]{1,0:T(1,128)} %bitcast.50, bf16[2048,512]{1,0:T(8,128)(2,1)} %recept_weight.1, bf16[2048,512]{1,0:T(8,128)(2,1)} %key_weight.1, bf16[2048,512]{1,0:T(8,128)(2,1)} %value_weight.1, ...), custom_call_target="tpu_custom_call" | custom-call | tf_op jit(solution)/shard_map/attention/pallas_call | solution.py:140
  30.2 40.5 %gather_tokens.1 = (bf16[32,2048]{1,0:T(8,128)(2,1)}, bf16[4,2,2,64,2048]{4,3,2,1,0:T(8,128)(2,1)}, f32[16,8,128]{2,1,0:T(8,128)}) custom-call(bf16[64,2048]{1,0:T(8,128)(2,1)} %get-tuple-element.7.partial, bf16[64,2048]{1,0:T(8,128)(2,1)} %hidden.3, f32[1,2048]{1,0:T(1,128)} %bitcast.51, f32[8,128]{1,0:T(8,128)} %select_maximum_fusion.meta), custom_call_target="tpu_custom_call" | custom-call | tf_op jit(solution)/shard_map/gather_tokens/pallas_call | solution.py:334
  70.7 0.0 copy-start.1
  70.7 0.0 copy-start.5
  70.7 0.0 copy-start.2
  70.7 3.4 %fusion.37 = f32[1,1024]{1,0:T(1,128)S(1)} fusion(bf16[1024,2048]{1,0:T(8,128)(2,1)} %bitcast.42, bf16[2048,1]{0,1:T(2,128)(2,1)} %reshape.32), kind=kOutput, calls=%fused_computation.43 | convolution fusion | flops 4194304 | bytes 4202496 | tf_op jit(solution)/shard_map/dot_general | solution.py:23
  74.1 0.0 copy-done.1
  74.2 0.1 broadcast_in_dim.51
  74.3 0.0 copy-done.5
  74.3 0.1 fusion.24
  74.4 0.1 eq.36
  74.5 0.2 select_reduce_fusion
  74.7 0.0 copy-start
  74.7 0.0 copy-start.3
  74.7 0.2 fusion.28
  74.9 0.0 copy-done.2
  75.0 3.9 %fusion.36 = f32[1024,176]{0,1:T(8,128)S(1)} fusion(bf16[1024,2048]{1,0:T(8,128)(2,1)} %bitcast.43, bf16[2048,176]{0,1:T(8,128)(2,1)S(1)} %copy-done.2), kind=kOutput, calls=%fused_computation.42 | convolution fusion | flops 738197504 | bytes 5636096 | tf_op jit(solution)/shard_map/dot_general | solution.py:19
  78.8 0.0 copy-done
  78.8 0.0 copy-done.3
  78.9 1.6 %fusion.22 = bf16[1024,176]{0,1:T(8,128)(2,1)S(1)} fusion(bf16[1024,2048]{1,0:T(8,128)(2,1)S(1)} %bitcast.44, bf16[2048,176]{0,1:T(8,128)(2,1)S(1)} %copy-done.3, f32[1024,176]{0,1:T(8,128)S(1)} %fusion.36, f32[1024]{0:T(1024)S(1)} %add_divide_fusion), kind=kOutput, calls=%fused_computation.17 | convolution fusion | flops 739278848 | bytes 6000640 | tf_op jit(solution)/shard_map/dot_general | solution.py:19
  80.5 1.3 convolution_convert_fusion.1
  81.8 0.2 copy.27
  82.0 3.8 %fusion.4 = f32[256,768]{1,0:T(8,128)} fusion(bf16[256,2048]{1,0:T(8,128)(2,1)S(1)} %convolution_convert_fusion.1, bf16[1,2048,768]{2,1,0:T(8,128)(2,1)} %param.43), kind=kOutput, calls=%fused_computation.5 | convolution fusion | flops 805306368 | bytes 4980736 | tf_op jit(solution)/shard_map/dot_general | solution.py:19
  85.7 0.0 copy-start.4
  85.8 6.3 %fusion.9 = bf16[256,2048]{1,0:T(8,128)(2,1)} fusion(bf16[1,768,2048]{2,1,0:T(8,128)(2,1)} %param.45, f32[256]{0:T(256)S(1)} %select_reduce_fusion, bf16[256,2048]{1,0:T(8,128)(2,1)S(1)} %convolution_convert_fusion.1, bf16[1,2048,768]{2,1,0:T(8,128)(2,1)} %param.44, f32[256,768]{1,0:T(8,128)} %fusion.4), kind=kOutput, calls=%fused_computation.8 | convolution fusion | flops 1612644352 | bytes 9176064 | tf_op jit(solution)/shard_map/dot_general | solution.py:19
  92.0 0.0 copy-done.4
  92.0 5.5 %convolution_convert_fusion = bf16[1024,2048]{1,0:T(8,128)(2,1)} fusion(bf16[176,2048]{1,0:T(8,128)(2,1)S(1)} %copy-done.4, bf16[256,2048]{1,0:T(8,128)(2,1)} %fusion.9, bf16[1024,176]{1,0:T(8,128)(2,1)S(1)} %copy.27, bf16[1024,256]{1,0:T(8,128)(2,1)S(1)} %fusion.28), kind=kOutput, calls=%fused_computation | convolution fusion | flops 1819344896 | bytes 6848512 | tf_op jit(solution)/shard_map/dot_general | solution.py:19
  97.5 34.5 %scatter_sum.1 = bf16[64,2048]{1,0:T(8,128)(2,1)} custom-call(bf16[4,2,2,64,2048]{4,3,2,1,0:T(8,128)(2,1)} %bitcast.46, bf16[32,2048]{1,0:T(8,128)(2,1)} %get-tuple-element.10.first), custom_call_target="tpu_custom_call" | custom-call | tf_op jit(solution)/shard_map/scatter_sum/pallas_call | solution.py:481
  132.1 1.7 %copy.29 = bf16[64,2048]{1,0:T(8,128)(2,1)} copy(bf16[64,2048]{1,0:T(8,128)(2,1)} %scatter_sum.1) | data formatting | bytes 524288
  (3 shorter events, 0.1 us)
Async XLA Ops:
  70.7 3.5 %copy-start.1 = (f32[16,8,128]{2,1,0:T(8,128)S(1)}, f32[16,8,128]{2,1,0:T(8,128)}, u32[]{:S(2)}) copy-start(f32[16,8,128]{2,1,0:T(8,128)} %get-tuple-element.8) | copy-start | bytes 196612
  70.7 3.6 %copy-start.5 = (s32[16]{0:T(128)S(1)}, s32[16]{0:T(128)}, u32[]{:S(2)}) copy-start(s32[16]{0:T(128)} %iota_multiply_fusion) | copy-start | bytes 196
  70.7 4.3 %copy-start.2 = (bf16[2048,176]{0,1:T(8,128)(2,1)S(1)}, bf16[2048,176]{0,1:T(8,128)(2,1)}, u32[]{:S(2)}) copy-start(bf16[2048,176]{0,1:T(8,128)(2,1)} %param.40) | copy-start | bytes 2162692
  74.7 4.1 %copy-start = (bf16[4,2,2,64,2048]{4,3,2,1,0:T(8,128)(2,1)S(1)}, bf16[4,2,2,64,2048]{4,3,2,1,0:T(8,128)(2,1)}, u32[]{:S(2)}) copy-start(bf16[4,2,2,64,2048]{4,3,2,1,0:T(8,128)(2,1)} %get-tuple-element.9) | copy-start | bytes 12582916
  74.7 4.1 %copy-start.3 = (bf16[2048,176]{0,1:T(8,128)(2,1)S(1)}, bf16[2048,176]{0,1:T(8,128)(2,1)}, u32[]{:S(2)}) copy-start(bf16[2048,176]{0,1:T(8,128)(2,1)} %param.41) | copy-start | bytes 2162692
  85.7 6.3 %copy-start.4 = (bf16[176,2048]{1,0:T(8,128)(2,1)S(1)}, bf16[176,2048]{1,0:T(8,128)(2,1)}, u32[]{:S(2)}) copy-start(bf16[176,2048]{1,0:T(8,128)(2,1)} %param.42) | copy-start | bytes 2162692
where the time goes:
time: 134 us
  Pallas kernels  101 us (75%)
  matrix products  25.8 us (19%)
  local copies, waits for them, and re-layouts  3.33 us (2%)
  other arithmetic  3.03 us (2%)
    pallas_call x1, Pallas kernels, gather_tokens(): pl.pallas_call(functools.partial(gather_kernel, sizes), out_shape=(jax.Sh...  40.5 us
    pallas_call x1, Pallas kernels, scatter_sum(): pl.pallas_call(functools.partial(scatter_kernel, sizes), out_shape=jax.Sh...  34.5 us
    pallas_call x1, Pallas kernels, attention(): pl.pallas_call(functools.partial(attention_kernel, step_rows), grid=(seqs...  25.7 us
    dot_general x7, matrix products, matmul(): return jnp.dot(left, right, preferred_element_type=F32)  22.4 us
    dot_general x1, matrix products, matmul_nt(): lax.dot_general(left, right, (((1,), (1,)), ((), ())), preferred_element_...  3.44 us
    unnamed x14, local copies, waits for them, and re-layouts  2.99 us

commit v1 on v0

--- a/solution.py
+++ b/solution.py
@@ -40,116 +40,161 @@
     return slow, mid, rest // mid
 
 
-def attention_kernel(
-    step_rows,
-    hidden,
-    mix_gain,
-    recept_weight,
-    key_weight,
-    value_weight,
-    decay_down,
-    decay_up,
-    decay_bias,
-    rate_down,
-    rate_up,
-    rate_bias,
-    head_gain,
-    out_weight,
-    state_in,
-    state_out,
-    partial,
-    recept_s,
-    unit_s,
-    unit_rate_s,
-    key_rate_s,
-    value_s,
-    decay_s,
-    readout_s,
-    normed_s,
-):
-    step = pl.program_id(0)
-    heads, seqs, size = recept_s.shape
+def attention_kernel(chunks, *refs):
+    sources, (state_h, state_out_h, partial), rest = refs[:13], refs[13:16], refs[16:]
+    local, rest = rest[:13], rest[13:]
+    state_v, new_v, recept_s, pull_s, key_rate_s, value_s, decay_s, readout_s, normed_s = rest[:9]
+    part_sem, in_sem, out_sem = rest[9:]
+    (
+        hidden,
+        mix_gain,
+        decay_down,
+        rate_down,
+        decay_up,
+        rate_up,
+        decay_bias,
+        rate_bias,
+        recept_weight,
+        key_weight,
+        value_weight,
+        head_gain,
+        out_weight,
+    ) = local
+    heads, seqs, size = pull_s.shape
     width = heads * size
+    step_rows = seqs // chunks
     own = pl.ds(pl.multiple_of(lax.axis_index("tp") * width, 128), width)
 
-    @pl.when(step == 0)
-    def _():
-        normed = rms_scaled(hidden[...].astype(F32), mix_gain[...]).astype(BF16)
-        recept = matmul(normed, recept_weight[...]).astype(BF16).astype(F32)
-        keys = matmul(normed, key_weight[...]).astype(BF16).astype(F32)
-        vals = matmul(normed, value_weight[...]).astype(BF16).astype(F32)
-        decay_low = jnp.tanh(matmul_nt(normed, decay_down[...])).astype(BF16)
-        decay_pre = matmul(decay_low, decay_up[:, own]) + decay_bias[:, own]
-        softplus = jnp.maximum(-decay_pre, 0.0) + jnp.log1p(jnp.exp(-jnp.abs(decay_pre)))
-        decay = jnp.exp(-jnp.exp(-softplus - 0.5))
-        rate_low = matmul_nt(normed, rate_down[...]).astype(BF16)
-        rate = 1.0 / (1.0 + jnp.exp(-(matmul(rate_low, rate_up[:, own]) + rate_bias[:, own])))
-        for h in range(heads):
-            cols = slice(h * size, (h + 1) * size)
-            key_h, rate_h = keys[:, cols], rate[:, cols]
-            unit = key_h * lax.rsqrt(jnp.sum(key_h * key_h, axis=-1, keepdims=True) + 1e-06)
-            recept_s[h] = recept[:, cols]
-            unit_s[h] = unit
-            unit_rate_s[h] = unit * rate_h
-            key_rate_s[h] = key_h * rate_h
-            value_s[h] = vals[:, cols]
-            decay_s[h] = decay[:, cols]
+    def part_copy(i):
+        return pltpu.make_async_copy(sources[i], local[i], part_sem.at[i])
+
+    def rows_of(c):
+        return pl.ds(c * step_rows, step_rows)
+
+    def in_copy(c):
+        return pltpu.make_async_copy(state_h.at[rows_of(c)], state_v.at[rows_of(c)], in_sem.at[c])
+
+    def out_copy(c):
+        return pltpu.make_async_copy(new_v.at[rows_of(c)], state_out_h.at[rows_of(c)], out_sem.at[c])
+
+    for i in range(11):
+        part_copy(i).start()
+
+    def start_in(c, carry):
+        in_copy(c).start()
+        return carry
+
+    lax.fori_loop(0, chunks, start_in, 0)
+    part_copy(11).start()
+    part_copy(12).start()
+
+    part_copy(0).wait()
+    part_copy(1).wait()
+    normed = rms_scaled(hidden[...].astype(F32), mix_gain[...]).astype(BF16)
+    for i in range(2, 8):
+        part_copy(i).wait()
+    decay_low = jnp.tanh(matmul_nt(normed, decay_down[...])).astype(BF16)
+    decay_pre = matmul(decay_low, decay_up[:, own]) + decay_bias[:, own]
+    decay = jnp.exp(-math.exp(-0.5) / (1.0 + jnp.exp(-decay_pre)))
+    rate_low = matmul_nt(normed, rate_down[...]).astype(BF16)
+    rate = 1.0 / (1.0 + jnp.exp(-(matmul(rate_low, rate_up[:, own]) + rate_bias[:, own])))
+    part_copy(8).wait()
+    recept = matmul(normed, recept_weight[...]).astype(BF16).astype(F32)
+    part_copy(9).wait()
+    keys = matmul(normed, key_weight[...]).astype(BF16).astype(F32)
+    part_copy(10).wait()
+    vals = matmul(normed, value_weight[...]).astype(BF16).astype(F32)
+    for h in range(heads):
+        cols = slice(h * size, (h + 1) * size)
+        key_h = keys[:, cols]
+        inverse = 1.0 / (jnp.sum(key_h * key_h, axis=-1, keepdims=True) + 1e-06)
+        recept_s[:, h, :] = recept[:, cols]
+        pull_s[h] = key_h * inverse
+        key_rate_s[h] = key_h * rate[:, cols]
+        value_s[h] = vals[:, cols]
+        decay_s[h] = decay[:, cols]
 
     shape, flat = (heads, size, size), (heads * size, size)
     eye = lax.broadcasted_iota(jnp.int32, shape, 1) == lax.broadcasted_iota(jnp.int32, shape, 2)
-    ones = jnp.ones((size, size), BF16)
-
-    def row_sums(values):
-        return matmul(values.astype(BF16).reshape(flat), ones).reshape(shape)
-
-    def one_sequence(local, carry):
-        row = pl.ds(step * step_rows + local, 1)
-        state = state_in[local]
-        removed = row_sums(state * unit_s[:, row])
-        value = row_sums(jnp.where(eye, value_s[:, row], 0.0))
-        new = (
-            state * decay_s[:, row] - removed * unit_rate_s[:, row] + value * key_rate_s[:, row]
+    spread = (heads, width)
+    owner = lax.broadcasted_iota(jnp.int32, spread, 0)
+    own_lanes = owner == lax.broadcasted_iota(jnp.int32, spread, 1) // size
+
+    def one_sequence(row):
+        here = pl.ds(row, 1)
+        state = state_v[row]
+        gain = jnp.sum(
+            jnp.where(eye, value_s[:, here], 0.0) - state * pull_s[:, here], axis=-1, keepdims=True
         )
-        state_out[local] = new
-        out = row_sums(new * recept_s[:, row])
-        readout_s[:, row] = jnp.sum(jnp.where(eye, out, 0.0), axis=1, keepdims=True)
+        new = state * decay_s[:, here] + gain * key_rate_s[:, here]
+        new_v[row] = new
+        out = matmul_nt(recept_s[row].astype(BF16), new.astype(BF16).reshape(flat))
+        readout_s[here, :] = jnp.sum(jnp.where(own_lanes, out, 0.0), axis=0, keepdims=True)
+
+    def one_chunk(c, carry):
+        in_copy(c).wait()
+
+        def some(k, inner):
+            for j in range(4):
+                one_sequence(c * step_rows + k * 4 + j)
+            return inner
+
+        lax.fori_loop(0, step_rows // 4, some, 0)
+        out_copy(c).start()
         return carry
 
-    lax.fori_loop(0, step_rows, one_sequence, 0, unroll=4)
-
-    @pl.when(step == pl.num_programs(0) - 1)
-    def _():
-        gain = head_gain[:, own]
-        for h in range(heads):
-            cols = slice(h * size, (h + 1) * size)
-            out = readout_s[h]
-            centred = out - jnp.mean(out, axis=-1, keepdims=True)
-            variance = jnp.mean(centred * centred, axis=-1, keepdims=True)
-            normed_s[:, cols] = (centred * lax.rsqrt(variance + 0.00064) * gain[:, cols]).astype(BF16)
-        partial[...] = matmul(normed_s[...], out_weight[...]).astype(BF16)
-
-
-def attention(hidden, vectors, state):
+    lax.fori_loop(0, chunks, one_chunk, 0)
+
+    part_copy(11).wait()
+    gain = head_gain[:, own]
+    for h in range(heads):
+        cols = slice(h * size, (h + 1) * size)
+        out = readout_s[:, cols]
+        centred = out - jnp.mean(out, axis=-1, keepdims=True)
+        variance = jnp.mean(centred * centred, axis=-1, keepdims=True)
+        normed_s[:, cols] = (centred * lax.rsqrt(variance + 0.00064) * gain[:, cols]).astype(BF16)
+    part_copy(12).wait()
+    partial[...] = matmul(normed_s[...], out_weight[...]).astype(BF16)
+
+    def wait_out(c, carry):
+        out_copy(c).wait()
+        return carry
+
+    lax.fori_loop(0, chunks, wait_out, 0)
+
+
+def attention(operands, state):
     seqs, heads, size, _ = state.shape
+    hidden = operands[0]
     width = heads * size
-    step_rows = math.gcd(seqs, 8)
-    block = pl.BlockSpec((step_rows, heads, size, size), lambda i: (i, 0, 0, 0))
-    operands = (hidden,) + vectors
-    whole = [pl.BlockSpec(a.shape, lambda i: (0, 0)) for a in operands]
+    chunks = seqs // math.gcd(seqs, 8)
     per_head = pltpu.VMEM((heads, seqs, size), F32)
+    dma = pltpu.SemaphoreType.DMA
+    any_spec = pl.BlockSpec(memory_space=pl.ANY)
     return pl.pallas_call(
-        functools.partial(attention_kernel, step_rows),
-        grid=(seqs // step_rows,),
+        functools.partial(attention_kernel, chunks),
         out_shape=(
             jax.ShapeDtypeStruct(state.shape, F32),
             jax.ShapeDtypeStruct(hidden.shape, BF16),
         ),
-        in_specs=whole + [block],
-        out_specs=(block, pl.BlockSpec(hidden.shape, lambda i: (0, 0))),
-        scratch_shapes=[per_head] * 7 + [pltpu.VMEM((seqs, width), BF16)],
-        compiler_params=pltpu.CompilerParams(
-            dimension_semantics=("arbitrary",), vmem_limit_bytes=VMEM_LIMIT
-        ),
+        in_specs=[any_spec] * 14,
+        out_specs=(any_spec, VMEM_SPEC),
+        scratch_shapes=[pltpu.VMEM(a.shape, a.dtype) for a in operands]
+        + [
+            pltpu.VMEM(state.shape, F32),
+            pltpu.VMEM(state.shape, F32),
+            pltpu.VMEM((seqs, heads, size), F32),
+            per_head,
+            per_head,
+            per_head,
+            per_head,
+            pltpu.VMEM((seqs, width), F32),
+            pltpu.VMEM((seqs, width), BF16),
+            dma((13,)),
+            dma((chunks,)),
+            dma((chunks,)),
+        ],
+        compiler_params=pltpu.CompilerParams(vmem_limit_bytes=VMEM_LIMIT),
         name="attention",
     )(*operands, state)
 
@@ -535,18 +580,18 @@
     top = routing.shape[1]
     cap = max(2, 2 * seqs * top // count)
     new_state, partial = attention(
-        hidden,
         (
+            hidden,
             mix_gain[None],
+            decay_down.T,
+            rate_down.T,
+            decay_up,
+            rate_up,
+            decay_bias[None],
+            rate_bias[None],
             recept_weight,
             key_weight,
             value_weight,
-            decay_down.T,
-            decay_up,
-            decay_bias[None],
-            rate_down.T,
-            rate_up,
-            rate_bias[None],
             head_gain[None],
             out_weight,
         ),

time: 134 us -> 124 us (0.925)
  Pallas kernels: 101 us -> 90.5 us
    pallas_call x1, Pallas kernels: 25.7 us -> 15.5 us  [attention(): pl.pallas_call(functools.partial(attention_kernel, chunks), out_shape=(ja...]
where the time goes in v1:
time: 124 us
  Pallas kernels  90.5 us (73%)
  matrix products  25.8 us (21%)
  local copies, waits for them, and re-layouts  3.33 us (3%)
  other arithmetic  3.03 us (2%)
    pallas_call x1, Pallas kernels, gather_tokens(): pl.pallas_call(functools.partial(gather_kernel, sizes), out_shape=(jax.Sh...  40.5 us
    pallas_call x1, Pallas kernels, scatter_sum(): pl.pallas_call(functools.partial(scatter_kernel, sizes), out_shape=jax.Sh...  34.6 us
    dot_general x7, matrix products, matmul(): return jnp.dot(left, right, preferred_element_type=F32)  22.4 us
    pallas_call x1, Pallas kernels, attention(): pl.pallas_call(functools.partial(attention_kernel, chunks), out_shape=(ja...  15.5 us
    dot_general x1, matrix products, matmul_nt(): lax.dot_general(left, right, (((1,), (1,)), ((), ())), preferred_element_...  3.44 us
    unnamed x14, local copies, waits for them, and re-layouts  2.99 us

profile of v1, /device:TPU:0, one launch (start us, length us, event | category | flops | bytes accessed | tf_op | source)
XLA Modules:
  0.0 123.5 jit_solution(9646586037499155064)
XLA Ops:
  0.6 0.5 iota_multiply_fusion
  1.2 0.7 convert_bitcast_fusion
  1.9 1.3 %select_maximum_fusion.meta = f32[8,128]{1,0:T(8,128)} fusion(f32[2,64]{1,0:T(2,128)} %bitcast.55, f32[2,64]{1,0:T(2,128)S(1)} %convert_bitcast_fusion), kind=kLoop, calls=%fused_computation.33 | loop fusion | flops 8192 | bytes 5120 | tf_op jit(solution)/shard_map/concatenate | solution.py:600
  3.1 1.3 %reshape.32 = bf16[2048,1]{0,1:T(2,128)(2,1)} reshape(bf16[2048]{0:T(1024)(128)(2,1)} %param.39) | data formatting | bytes 8192 | tf_op args[15]
  4.4 15.5 %attention.1 = (f32[64,8,64,64]{3,2,1,0:T(8,128)}, bf16[64,2048]{1,0:T(8,128)(2,1)}) custom-call(bf16[64,2048]{1,0:T(8,128)(2,1)} %hidden.1, f32[1,2048]{1,0:T(1,128)} %bitcast.50, bf16[64,2048]{1,0:T(8,128)(2,1)} %bitcast.47, bf16[64,2048]{1,0:T(8,128)(2,1)} %bitcast.48, bf16[64,1024]{1,0:T(8,128)(2,1)} %refs_4_.1, bf16[64,1024]{1,0:T(8,128)(2,1)} %refs_5_.1, ...), custom_call_target="tpu_custom_call" | custom-call | tf_op jit(solution)/shard_map/attention/pallas_call | solution.py:174
  19.9 40.5 %gather_tokens.1 = (bf16[32,2048]{1,0:T(8,128)(2,1)}, bf16[4,2,2,64,2048]{4,3,2,1,0:T(8,128)(2,1)}, f32[16,8,128]{2,1,0:T(8,128)}) custom-call(bf16[64,2048]{1,0:T(8,128)(2,1)} %get-tuple-element.7.partial, bf16[64,2048]{1,0:T(8,128)(2,1)} %hidden.1, f32[1,2048]{1,0:T(1,128)} %bitcast.51, f32[8,128]{1,0:T(8,128)} %select_maximum_fusion.meta), custom_call_target="tpu_custom_call" | custom-call | tf_op jit(solution)/shard_map/gather_tokens/pallas_call | solution.py:379
  60.4 0.0 copy-start.1
  60.4 0.0 copy-start.5
  60.4 0.0 copy-start.2
  60.5 3.4 %fusion.37 = f32[1,1024]{1,0:T(1,128)S(1)} fusion(bf16[1024,2048]{1,0:T(8,128)(2,1)} %bitcast.42, bf16[2048,1]{0,1:T(2,128)(2,1)} %reshape.32), kind=kOutput, calls=%fused_computation.43 | convolution fusion | flops 4194304 | bytes 4202496 | tf_op jit(solution)/shard_map/dot_general | solution.py:23
  63.9 0.0 copy-done.1
  64.0 0.1 broadcast_in_dim.51
  64.1 0.0 copy-done.5
  64.1 0.1 fusion.24
  64.2 0.1 eq.36
  64.2 0.2 select_reduce_fusion
  64.5 0.0 copy-start
  64.5 0.0 copy-start.3
  64.5 0.2 fusion.28
  64.7 0.0 copy-done.2
  64.7 3.9 %fusion.36 = f32[1024,176]{0,1:T(8,128)S(1)} fusion(bf16[1024,2048]{1,0:T(8,128)(2,1)} %bitcast.43, bf16[2048,176]{0,1:T(8,128)(2,1)S(1)} %copy-done.2), kind=kOutput, calls=%fused_computation.42 | convolution fusion | flops 738197504 | bytes 5636096 | tf_op jit(solution)/shard_map/dot_general | solution.py:19
  68.6 0.0 copy-done
  68.6 0.0 copy-done.3
  68.6 1.6 %fusion.22 = bf16[1024,176]{0,1:T(8,128)(2,1)S(1)} fusion(bf16[1024,2048]{1,0:T(8,128)(2,1)S(1)} %bitcast.44, bf16[2048,176]{0,1:T(8,128)(2,1)S(1)} %copy-done.3, f32[1024,176]{0,1:T(8,128)S(1)} %fusion.36, f32[1024]{0:T(1024)S(1)} %add_divide_fusion), kind=kOutput, calls=%fused_computation.17 | convolution fusion | flops 739278848 | bytes 6000640 | tf_op jit(solution)/shard_map/dot_general | solution.py:19
  70.2 1.3 %convolution_convert_fusion.1 = bf16[256,2048]{1,0:T(8,128)(2,1)S(1)} fusion(bf16[1024,2048]{1,0:T(8,128)(2,1)S(1)} %bitcast.45, s32[1024]{0:T(1024)S(1)} %eq.36), kind=kOutput, calls=%fused_computation.9 | convolution fusion | flops 1074528256 | bytes 5246976 | tf_op jit(solution)/shard_map/dot_general | solution.py:19
  71.5 0.2 copy.27
  71.7 3.8 %fusion.4 = f32[256,768]{1,0:T(8,128)} fusion(bf16[256,2048]{1,0:T(8,128)(2,1)S(1)} %convolution_convert_fusion.1, bf16[1,2048,768]{2,1,0:T(8,128)(2,1)} %param.43), kind=kOutput, calls=%fused_computation.5 | convolution fusion | flops 805306368 | bytes 4980736 | tf_op jit(solution)/shard_map/dot_general | solution.py:19
  75.5 0.0 copy-start.4
  75.5 6.3 %fusion.9 = bf16[256,2048]{1,0:T(8,128)(2,1)} fusion(bf16[1,768,2048]{2,1,0:T(8,128)(2,1)} %param.45, f32[256]{0:T(256)S(1)} %select_reduce_fusion, bf16[256,2048]{1,0:T(8,128)(2,1)S(1)} %convolution_convert_fusion.1, bf16[1,2048,768]{2,1,0:T(8,128)(2,1)} %param.44, f32[256,768]{1,0:T(8,128)} %fusion.4), kind=kOutput, calls=%fused_computation.8 | convolution fusion | flops 1612644352 | bytes 9176064 | tf_op jit(solution)/shard_map/dot_general | solution.py:19
  81.8 0.0 copy-done.4
  81.8 5.5 %convolution_convert_fusion = bf16[1024,2048]{1,0:T(8,128)(2,1)} fusion(bf16[176,2048]{1,0:T(8,128)(2,1)S(1)} %copy-done.4, bf16[256,2048]{1,0:T(8,128)(2,1)} %fusion.9, bf16[1024,176]{1,0:T(8,128)(2,1)S(1)} %copy.27, bf16[1024,256]{1,0:T(8,128)(2,1)S(1)} %fusion.28), kind=kOutput, calls=%fused_computation | convolution fusion | flops 1819344896 | bytes 6848512 | tf_op jit(solution)/shard_map/dot_general | solution.py:19
  87.3 34.6 %scatter_sum.1 = bf16[64,2048]{1,0:T(8,128)(2,1)} custom-call(bf16[4,2,2,64,2048]{4,3,2,1,0:T(8,128)(2,1)} %bitcast.46, bf16[32,2048]{1,0:T(8,128)(2,1)} %get-tuple-element.10.first), custom_call_target="tpu_custom_call" | custom-call | tf_op jit(solution)/shard_map/scatter_sum/pallas_call | solution.py:526
  121.9 1.7 %copy.29 = bf16[64,2048]{1,0:T(8,128)(2,1)} copy(bf16[64,2048]{1,0:T(8,128)(2,1)} %scatter_sum.1) | data formatting | bytes 524288
  (3 shorter events, 0.1 us)
Async XLA Ops:
  60.4 3.5 %copy-start.1 = (f32[16,8,128]{2,1,0:T(8,128)S(1)}, f32[16,8,128]{2,1,0:T(8,128)}, u32[]{:S(2)}) copy-start(f32[16,8,128]{2,1,0:T(8,128)} %get-tuple-element.8) | copy-start | bytes 196612
  60.4 3.6 %copy-start.5 = (s32[16]{0:T(128)S(1)}, s32[16]{0:T(128)}, u32[]{:S(2)}) copy-start(s32[16]{0:T(128)} %iota_multiply_fusion) | copy-start | bytes 196
  60.4 4.3 %copy-start.2 = (bf16[2048,176]{0,1:T(8,128)(2,1)S(1)}, bf16[2048,176]{0,1:T(8,128)(2,1)}, u32[]{:S(2)}) copy-start(bf16[2048,176]{0,1:T(8,128)(2,1)} %param.40) | copy-start | bytes 2162692
  64.5 4.1 %copy-start = (bf16[4,2,2,64,2048]{4,3,2,1,0:T(8,128)(2,1)S(1)}, bf16[4,2,2,64,2048]{4,3,2,1,0:T(8,128)(2,1)}, u32[]{:S(2)}) copy-start(bf16[4,2,2,64,2048]{4,3,2,1,0:T(8,128)(2,1)} %get-tuple-element.9) | copy-start | bytes 12582916
  64.5 4.1 %copy-start.3 = (bf16[2048,176]{0,1:T(8,128)(2,1)S(1)}, bf16[2048,176]{0,1:T(8,128)(2,1)}, u32[]{:S(2)}) copy-start(bf16[2048,176]{0,1:T(8,128)(2,1)} %param.41) | copy-start | bytes 2162692
  75.5 6.3 %copy-start.4 = (bf16[176,2048]{1,0:T(8,128)(2,1)S(1)}, bf16[176,2048]{1,0:T(8,128)(2,1)}, u32[]{:S(2)}) copy-start(bf16[176,2048]{1,0:T(8,128)(2,1)} %param.42) | copy-start | bytes 2162692

commit v2 on v1

v2 whole, which is shorter than its diff:
```python
import functools
import math

import jax
import jax.numpy as jnp
from jax import lax
from jax.experimental import pallas as pl
from jax.experimental.pallas import tpu as pltpu
from jax.sharding import PartitionSpec as P

MESH = pl.DeviceIdType.MESH
F32 = jnp.float32
BF16 = jnp.bfloat16
VMEM_LIMIT = 64 * 1024 * 1024 - 65536
VMEM_SPEC = pl.BlockSpec(memory_space=pltpu.VMEM)


def matmul(left, right):
    return jnp.dot(left, right, preferred_element_type=F32)


def matmul_nt(left, right):
    return lax.dot_general(left, right, (((1,), (1,)), ((), ())), preferred_element_type=F32)


def silu_of(tensor):
    return tensor / (1.0 + jnp.exp(-tensor))


def rms_scaled(values, gain):
    return values * lax.rsqrt(jnp.mean(values * values, axis=-1, keepdims=True) + 1e-06) * gain


def factors_of(count):
    slow = 4 if count % 4 == 0 else 1
    rest = count // slow
    mid = math.isqrt(rest)
    while rest % mid:
        mid -= 1
    return slow, mid, rest // mid


def attention_kernel(chunks, *refs):
    sources, (state_h, state_out_h, partial), rest = refs[:13], refs[13:16], refs[16:]
    local, rest = rest[:13], rest[13:]
    state_v, new_v, recept_s, pull_s, key_rate_s, value_s, decay_s, readout_s, normed_s = rest[:9]
    part_sem, in_sem, out_sem = rest[9:]
    (
        hidden,
        mix_gain,
        decay_down,
        rate_down,
        decay_up,
        rate_up,
        decay_bias,
        rate_bias,
        recept_weight,
        key_weight,
        value_weight,
        head_gain,
        out_weight,
    ) = local
    heads, seqs, size = pull_s.shape
    width = heads * size
    step_rows = seqs // chunks
    own = pl.ds(pl.multiple_of(lax.axis_index("tp") * width, 128), width)

    def part_copy(i):
        return pltpu.make_async_copy(sources[i], local[i], part_sem.at[i])

    def rows_of(c):
        return pl.ds(c * step_rows, step_rows)

    def in_copy(c):
        return pltpu.make_async_copy(state_h.at[rows_of(c)], state_v.at[rows_of(c)], in_sem.at[c])

    def out_copy(c):
        return pltpu.make_async_copy(new_v.at[rows_of(c)], state_out_h.at[rows_of(c)], out_sem.at[c])

    for i in range(11):
        part_copy(i).start()

    def start_in(c, carry):
        in_copy(c).start()
        return carry

    lax.fori_loop(0, chunks, start_in, 0)
    part_copy(11).start()
    part_copy(12).start()

    part_copy(0).wait()
    part_copy(1).wait()
    normed = rms_scaled(hidden[...].astype(F32), mix_gain[...]).astype(BF16)
    for i in range(2, 8):
        part_copy(i).wait()
    decay_low = jnp.tanh(matmul_nt(normed, decay_down[...])).astype(BF16)
    decay_pre = matmul(decay_low, decay_up[:, own]) + decay_bias[:, own]
    decay = jnp.exp(-math.exp(-0.5) / (1.0 + jnp.exp(-decay_pre)))
    rate_low = matmul_nt(normed, rate_down[...]).astype(BF16)
    rate = 1.0 / (1.0 + jnp.exp(-(matmul(rate_low, rate_up[:, own]) + rate_bias[:, own])))
    part_copy(8).wait()
    recept = matmul(normed, recept_weight[...]).astype(BF16).astype(F32)
    part_copy(9).wait()
    keys = matmul(normed, key_weight[...]).astype(BF16).astype(F32)
    part_copy(10).wait()
    vals = matmul(normed, value_weight[...]).astype(BF16).astype(F32)
    for h in range(heads):
        cols = slice(h * size, (h + 1) * size)
        key_h = keys[:, cols]
        inverse = 1.0 / (jnp.sum(key_h * key_h, axis=-1, keepdims=True) + 1e-06)
        recept_s[:, h, :] = recept[:, cols]
        pull_s[h] = key_h * inverse
        key_rate_s[h] = key_h * rate[:, cols]
        value_s[h] = vals[:, cols]
        decay_s[h] = decay[:, cols]

    shape, flat = (heads, size, size), (heads * size, size)
    eye = lax.broadcasted_iota(jnp.int32, shape, 1) == lax.broadcasted_iota(jnp.int32, shape, 2)
    spread = (heads, width)
    owner = lax.broadcasted_iota(jnp.int32, spread, 0)
    own_lanes = owner == lax.broadcasted_iota(jnp.int32, spread, 1) // size

    def one_sequence(row):
        here = pl.ds(row, 1)
        state = state_v[row]
        gain = jnp.sum(
            jnp.where(eye, value_s[:, here], 0.0) - state * pull_s[:, here], axis=-1, keepdims=True
        )
        new = state * decay_s[:, here] + gain * key_rate_s[:, here]
        new_v[row] = new
        out = matmul_nt(recept_s[row].astype(BF16), new.astype(BF16).reshape(flat))
        readout_s[here, :] = jnp.sum(jnp.where(own_lanes, out, 0.0), axis=0, keepdims=True)

    def one_chunk(c, carry):
        in_copy(c).wait()

        def some(k, inner):
            for j in range(4):
                one_sequence(c * step_rows + k * 4 + j)
            return inner

        lax.fori_loop(0, step_rows // 4, some, 0)
        out_copy(c).start()
        return carry

    lax.fori_loop(0, chunks, one_chunk, 0)

    part_copy(11).wait()
    gain = head_gain[:, own]
    for h in range(heads):
        cols = slice(h * size, (h + 1) * size)
        out = readout_s[:, cols]
        centred = out - jnp.mean(out, axis=-1, keepdims=True)
        variance = jnp.mean(centred * centred, axis=-1, keepdims=True)
        normed_s[:, cols] = (centred * lax.rsqrt(variance + 0.00064) * gain[:, cols]).astype(BF16)
    part_copy(12).wait()
    partial[...] = matmul(normed_s[...], out_weight[...]).astype(BF16)

    def wait_out(c, carry):
        out_copy(c).wait()
        return carry

    lax.fori_loop(0, chunks, wait_out, 0)


def attention(operands, state):
    seqs, heads, size, _ = state.shape
    hidden = operands[0]
    width = heads * size
    chunks = seqs // math.gcd(seqs, 8)
    per_head = pltpu.VMEM((heads, seqs, size), F32)
    dma = pltpu.SemaphoreType.DMA
    any_spec = pl.BlockSpec(memory_space=pl.ANY)
    return pl.pallas_call(
        functools.partial(attention_kernel, chunks),
        out_shape=(
            jax.ShapeDtypeStruct(state.shape, F32),
            jax.ShapeDtypeStruct(hidden.shape, BF16),
        ),
        in_specs=[any_spec] * 14,
        out_specs=(any_spec, VMEM_SPEC),
        scratch_shapes=[pltpu.VMEM(a.shape, a.dtype) for a in operands]
        + [
            pltpu.VMEM(state.shape, F32),
            pltpu.VMEM(state.shape, F32),
            pltpu.VMEM((seqs, heads, size), F32),
            per_head,
            per_head,
            per_head,
            per_head,
            pltpu.VMEM((seqs, width), F32),
            pltpu.VMEM((seqs, width), BF16),
            dma((13,)),
            dma((chunks,)),
            dma((chunks,)),
        ],
        compiler_params=pltpu.CompilerParams(vmem_limit_bytes=VMEM_LIMIT),
        name="attention",
    )(*operands, state)


def position(sizes):
    ep = lax.axis_index("ep")
    strides = (sizes[1] * sizes[2], sizes[2], 1)
    return ep, tuple(ep // s % n for s, n in zip(strides, sizes)), strides


def greet_all(count):
    ep, tp = lax.axis_index("ep"), lax.axis_index("tp")
    barrier = pltpu.get_barrier_semaphore()

    def greet(k, carry):
        pl.semaphore_signal(
            barrier, inc=1, device_id=((ep + k) % count, tp), device_id_type=MESH
        )
        return carry

    lax.fori_loop(1, count, greet, 0)
    pl.semaphore_signal(barrier, inc=1, device_id=(ep, 1 - tp), device_id_type=MESH)
    pl.semaphore_wait(barrier, count)


def remote(src, dst, send, recv, device):
    return pltpu.make_async_remote_copy(
        src_ref=src,
        dst_ref=dst,
        send_sem=send,
        recv_sem=recv,
        device_id=device,
        device_id_type=MESH,
    )


def layer_kernel(
    sizes,
    top,
    cap,
    partial,
    hidden,
    gain,
    blend_vector,
    routing,
    route_scale,
    gate_h,
    up_h,
    down_h,
    expert_gate_h,
    expert_up_h,
    expert_down_h,
    out,
    tokens,
    metas,
    meta,
    first,
    sibling_part,
    gate_v,
    up_v,
    down_v,
    expert_gate,
    expert_up,
    expert_down,
    gate_w,
    up_w,
    mix_w,
    mix_rows,
    picked,
    expert_act,
    slot_scale,
    from_sibling,
    lands,
    sems,
):
    (
        weight_sem,
        part_sem,
        meta_send,
        meta_recv,
        ag_send,
        ag_recv,
        pass_send,
        pass_recv,
        pair_send,
        pair_recv,
        rs_send,
        rs_recv,
        last_sem,
    ) = sems
    chunks, across, along = sizes
    count = chunks * across * along
    plane = across * along
    ep, at, strides = position(sizes)
    tp = lax.axis_index("tp")
    half, width = first.shape
    seqs = 2 * half
    sibling = (ep, 1 - tp)
    mine = pl.ds(pl.multiple_of(tp * half, half), half)
    other = pl.ds(pl.multiple_of((1 - tp) * half, half), half)
    slots = plane * cap
    depth = gate_w.shape[0]
    units = gate_v.shape[0]
    rows_at_once = max(1, 256 // (along * seqs))
    blocks = across // rows_at_once
    block_chips = rows_at_once * along
    block_rows = block_chips * seqs
    tile = 256

    weights = (
        (gate_h, gate_v),
        (up_h, up_v),
        (down_h, down_v),
        (expert_gate_h, expert_gate),
        (expert_up_h, expert_up),
        (expert_down_h, expert_down),
    )

    def weight_copy(i):
        return pltpu.make_async_copy(weights[i][0], weights[i][1], weight_sem.at[i])

    def per_core(run):
        @pl.when(tp == 0)
        def _():
            run(0)

        @pl.when(tp == 1)
        def _():
            run(1)

    def meta_copy(k):
        peer = (ep + k) % count
        place = metas.at[at[0], at[1] * along + at[2]]
        return remote(meta, place, meta_send.at[k], meta_recv.at[k], (peer, tp))

    for i in range(6):
        weight_copy(i).start()
    greet_all(count)
    swap = remote(partial.at[other], sibling_part, part_sem.at[0], part_sem.at[1], sibling)
    swap.start()
    meta[...] = jnp.zeros(meta.shape, F32)
    meta[0:top, 0:seqs] = routing[...].astype(F32)
    meta[top : 2 * top, 0:seqs] = route_scale[...]
    base = hidden[mine, :].astype(F32) + partial[mine, :].astype(F32)
    swap.wait()
    total = (base + sibling_part[...].astype(F32)).astype(BF16)
    first[...] = total
    tokens[at[0], at[1], at[2], mine, :] = rms_scaled(total.astype(F32), gain[...]).astype(BF16)

    gather_orders = ((0, 2, 1), (0, 1, 2))

    def gather_view(core, stage, k, j):
        _, d2, d3 = gather_orders[core]
        spot = [pl.ds((at[0] + chunks - k) % chunks, 1), None, None]

        def one(d, back=0):
            return pl.ds((at[d] + sizes[d] - back) % sizes[d], 1)

        spot[d2] = pl.ds(0, sizes[d2]) if stage == 2 else one(d2, j if stage == 1 else 0)
        spot[d3] = one(d3, j if stage == 2 else 0)
        return tokens.at[tuple(spot) + (pl.ds(core * half, half),)]

    def gather_copy(core, stage, k, j):
        d = gather_orders[core][stage]
        source = gather_view(core, stage, 0 if stage == 0 else k, 0)
        peer = ep + ((at[d] + j) % sizes[d] - at[d]) * strides[d]
        slot = (stage, k, j if stage else 0)
        return remote(source, source, ag_send.at[slot], ag_recv.at[slot], (peer, core))

    def pass_copy(core, stage, k, j):
        view, slot = gather_view(core, stage, k, j), (stage, k, j)
        return remote(view, view, pass_send.at[slot], pass_recv.at[slot], sibling)

    def pass_slots(core, k):
        yield 0, k, 0
        for stage in (1, 2):
            for j in range(1, sizes[gather_orders[core][stage]]):
                yield stage, k, j

    def gather_begin(core):
        for j in range(1, sizes[gather_orders[core][1]]):
            gather_copy(core, 1, 0, j).start()
        for k in range(1, chunks):
            gather_copy(core, 0, k, k).start()
        pass_copy(core, 0, 0, 0).start()

    def gather_step(core, t):
        order = gather_orders[core]

        def later_phase(stage, k):
            for j in range(1, sizes[order[stage]]):
                gather_copy(core, stage, k, j).wait()
            if stage == 1:
                for j in range(1, sizes[order[2]]):
                    gather_copy(core, 2, k, j).start()
            for j in range(1, sizes[order[stage]]):
                pass_copy(core, stage, k, j).start()

        if 0 <= t - 1 < chunks:
            later_phase(1, t - 1)
        if 0 < t < chunks:
            gather_copy(core, 0, t, t).wait()
            for j in range(1, sizes[order[1]]):
                gather_copy(core, 1, t, j).start()
            pass_copy(core, 0, t, 0).start()
        if 0 <= t - 2 < chunks:
            later_phase(2, t - 2)

    per_core(gather_begin)

    def start_meta(k, carry):
        meta_copy(k).start()
        return carry

    def wait_meta(k, carry):
        meta_copy(k).wait()
        return carry

    lax.fori_loop(1, count, start_meta, 0)
    metas[at[0], at[1] * along + at[2]] = meta[...]

    for i in range(3):
        weight_copy(i).wait()
    top_row = lax.broadcasted_iota(jnp.int32, (slots, width), 0) == 0
    gate_w[0:slots, :] = jnp.where(top_row, blend_vector[...].astype(F32), 0.0).astype(BF16)
    up_w[0:slots, :] = jnp.zeros((slots, width), BF16)
    if slots + units < depth:
        rest = (depth - slots - units, width)
        gate_w[slots + units : depth, :] = jnp.zeros(rest, BF16)
        up_w[slots + units : depth, :] = jnp.zeros(rest, BF16)
    gate_w[slots : slots + units, :] = gate_v[...]
    up_w[slots : slots + units, :] = up_v[...]

    def fill(z, carry):
        if slots + units < depth:
            mix_w[z, slots + units : depth, :] = jnp.zeros((depth - slots - units, width), BF16)
        mix_w[z, slots : slots + units, :] = down_v[...]
        return carry

    lax.fori_loop(0, chunks, fill, 0)

    def plane_of(k):
        return (at[0] + chunks - k) % chunks

    def use_tokens(k):
        z = plane_of(k)

        def arrive(core):
            for slot in pass_slots(1 - core, k):
                pass_copy(1 - core, *slot).wait_recv()

        per_core(arrive)
        here = metas[z]
        lanes = lax.broadcasted_iota(jnp.int32, (plane, 128), 1)
        expert = ep.astype(F32)
        chosen = jnp.zeros((plane, 128), F32)
        scale_of = jnp.zeros((plane, 128), F32)
        for c in range(top):
            hit = jnp.where((here[:, c, :] == expert) & (lanes < seqs), 1.0, 0.0)
            chosen = chosen + hit
            scale_of = scale_of + hit * here[:, top + c, :]
        earlier = lax.broadcasted_iota(jnp.int32, (128, 128), 0) < lax.broadcasted_iota(
            jnp.int32, (128, 128), 1
        )
        rank = matmul(chosen.astype(BF16), jnp.where(earlier, 1.0, 0.0).astype(BF16))
        chip = lax.broadcasted_iota(jnp.int32, (plane, 128), 0).astype(F32)
        place = jnp.where(chosen > 0.5, rank + chip * cap, -1.0)
        scales = jnp.zeros((slots, 1), F32)
        for i in range(blocks):
            chips = range(i * block_chips, (i + 1) * block_chips)
            place_row = jnp.concatenate([place[p : p + 1, :seqs] for p in chips], axis=1)
            scale_row = jnp.concatenate([scale_of[p : p + 1, :seqs] for p in chips], axis=1)
            slot_of = lax.broadcasted_iota(jnp.int32, (depth, block_rows), 0).astype(F32)
            select = jnp.where(slot_of == place_row, 1.0, 0.0)
            scales = scales + jnp.sum(select[:slots] * scale_row, axis=1, keepdims=True)
            ys = pl.ds(i * rows_at_once, rows_at_once)
            own_slots = slice(i * block_chips * cap, (i + 1) * block_chips * cap)
            part = select[own_slots].astype(BF16)

            def pick(n, carry):
                cols = pl.ds(pl.multiple_of(n * tile, tile), tile)
                found = matmul(part, tokens[z, ys, :, :, cols].reshape(block_rows, tile))
                picked[z, own_slots, cols] = found.astype(BF16)
                return carry

            lax.fori_loop(0, width // tile, pick, 0)
            own_rows = slice(i * block_rows, (i + 1) * block_rows)
            mix_rows[z, own_rows, :] = jnp.transpose(select).astype(BF16)
        slot_scale[z] = jnp.broadcast_to(scales, (slots, 128))

        def dense(i, carry):
            rows = tokens[z, pl.ds(i * rows_at_once, rows_at_once)].reshape(block_rows, width)
            gate = matmul_nt(rows, gate_w[...])
            blend = 1.0 / (1.0 + jnp.exp(-gate[:, 0:1]))
            act = silu_of(gate) * matmul_nt(rows, up_w[...]) * blend
            own_rows = pl.ds(pl.multiple_of(i * block_rows, block_rows), block_rows)
            mix_rows[z, own_rows, :] = (mix_rows[z, own_rows, :].astype(F32) + act).astype(BF16)
            return carry

        lax.fori_loop(0, blocks, dense, 0)

    for t in range(chunks + 2):
        per_core(functools.partial(gather_step, t=t))
        if t == 2:
            lax.fori_loop(1, count, wait_meta, 0)
        if t >= 3:
            use_tokens(t - 3)
    use_tokens(chunks - 1)

    def passes_done(core):
        for k in range(chunks):
            for slot in pass_slots(core, k):
                pass_copy(core, *slot).wait_send()

    per_core(passes_done)

    for i in range(3, 6):
        weight_copy(i).wait()
    slots_all = chunks * slots

    def expert_hidden(n, carry):
        cols = pl.ds(pl.multiple_of(n * tile, tile), tile)
        rows = picked[...].reshape(slots_all, width)
        gate = matmul(rows, expert_gate[0, :, cols])
        expert_act[:, cols] = (silu_of(gate) * matmul(rows, expert_up[0, :, cols])).astype(BF16)
        return carry

    lax.fori_loop(0, expert_gate.shape[2] // tile, expert_hidden, 0)
    scale_all = slot_scale[...].reshape(slots_all, 128)[:, 0:1]

    def expert_result(n, carry):
        cols = pl.ds(pl.multiple_of(n * tile, tile), tile)
        result = (matmul(expert_act[...], expert_down[0, :, cols]) * scale_all).astype(BF16)
        for z in range(chunks):
            mix_w[z, 0:slots, cols] = result[z * slots : (z + 1) * slots]
        return carry

    lax.fori_loop(0, width // tile, expert_result, 0)

    goals = [(at[0] + 1 + k) % chunks for k in range(chunks)]
    scatter_orders = ((1, 2), (2, 1))

    def pair_copy(k):
        return remote(
            tokens.at[goals[k], :, :, other],
            from_sibling.at[k],
            pair_send.at[k],
            pair_recv.at[k],
            sibling,
        )

    def make_part(k):
        z = goals[k]

        def some(n, carry):
            cols = pl.ds(pl.multiple_of(n * tile, tile), tile)
            for i in range(blocks):
                own_rows = slice(i * block_rows, (i + 1) * block_rows)
                part = matmul(mix_rows[z, own_rows, :], mix_w[z, :, cols]).astype(BF16)
                ys = pl.ds(i * rows_at_once, rows_at_once)
                tokens[z, ys, :, :, cols] = part.reshape(rows_at_once, along, seqs, tile)
            return carry

        lax.fori_loop(0, width // tile, some, 0)
        pair_copy(k).start()

    def spot(core, k, c1, c2):
        d1, d2 = scatter_orders[core]
        place = [goals[k], None, None]
        place[d1], place[d2] = c1, c2
        return tuple(place) + (pl.ds(core * half, half),)

    def scatter_copy(core, stage, k, j):
        d1, d2 = scatter_orders[core]
        if stage == 0:
            d = d1
            source = tokens.at[spot(core, k, (at[d1] + j) % sizes[d1], slice(None))]
            target = lands[0].at[k, j - 1]
        elif stage == 1:
            d = d2
            source = tokens.at[spot(core, k, at[d1], (at[d2] + j) % sizes[d2])]
            target = lands[1].at[k, j - 1]
        else:
            d = 0
            source = tokens.at[spot(core, k, at[d1], at[d2])]
            target = lands[2].at[k]
        peer = ep + ((at[d] + j) % sizes[d] - at[d]) * strides[d]
        slot = (stage, k, j if stage < 2 else 0)
        return remote(source, target, rs_send.at[slot], rs_recv.at[slot], (peer, core))

    def pair_sum(k):
        pair_copy(k).wait()

        def add(b, carry):
            y, x = b // along, b % along
            tokens[goals[k], y, x, mine, :] = (
                tokens[goals[k], y, x, mine, :].astype(F32) + from_sibling[k, y, x].astype(F32)
            ).astype(BF16)
            return carry

        lax.fori_loop(0, plane, add, 0)

        def send(core):
            for j in range(1, sizes[scatter_orders[core][0]]):
                scatter_copy(core, 0, k, j).start()

        per_core(send)

    def first_sum(core, k):
        d1, d2 = scatter_orders[core]
        for j in range(1, sizes[d1]):
            scatter_copy(core, 0, k, j).wait()

        def add(b, carry):
            place = spot(core, k, at[d1], b)
            value = tokens[place].astype(F32)
            for j in range(1, sizes[d1]):
                value = value + lands[0][k, j - 1, b].astype(F32)
            tokens[place] = value.astype(BF16)
            return carry

        lax.fori_loop(0, sizes[d2], add, 0)
        for j in range(1, sizes[d2]):
            scatter_copy(core, 1, k, j).start()

    def second_sum(core, k):
        d1, d2 = scatter_orders[core]
        for j in range(1, sizes[d2]):
            scatter_copy(core, 1, k, j).wait()
        place = spot(core, k, at[d1], at[d2])
        value = tokens[place].astype(F32)
        for j in range(1, sizes[d2]):
            value = value + lands[1][k, j - 1].astype(F32)
        if k < chunks - 1:
            tokens[place] = value.astype(BF16)
            scatter_copy(core, 2, k, k + 1).start()
            return
        value = value + first[...].astype(F32)
        for i in range(chunks - 1):
            scatter_copy(core, 2, i, i + 1).wait()
            value = value + lands[2][i].astype(F32)
        out[pl.ds(core * half, half), :] = value.astype(BF16)

    for t in range(chunks + 3):
        if t < chunks:
            make_part(t)
        if 0 <= t - 1 < chunks:
            pair_sum(t - 1)
        if 0 <= t - 2 < chunks:
            per_core(functools.partial(first_sum, k=t - 2))
        if 0 <= t - 3 < chunks:
            per_core(functools.partial(second_sum, k=t - 3))

    last = remote(out.at[mine], out.at[mine], last_sem.at[0], last_sem.at[1], sibling)
    last.start()
    last.wait()


def layer_after(sizes, partial, hidden, gain, blend_vector, routing, route_scale, weights):
    seqs, width = hidden.shape
    count = sizes[0] * sizes[1] * sizes[2]
    half, top, most = seqs // 2, routing.shape[0], max(sizes)
    cap = max(2, 2 * seqs * top // count)
    plane = sizes[1] * sizes[2]
    slots = plane * cap
    depth = -(-(slots + weights[0].shape[0]) // 128) * 128
    chunks, side, block = sizes[0], max(sizes[1:]), (half, width)
    dma = pltpu.SemaphoreType.DMA
    any_spec = pl.BlockSpec(memory_space=pl.ANY)
    hop = dma((3, chunks, most))
    return pl.pallas_call(
        functools.partial(layer_kernel, sizes, top, cap),
        out_shape=jax.ShapeDtypeStruct((seqs, width), BF16),
        in_specs=[VMEM_SPEC] * 6 + [any_spec] * 6,
        out_specs=VMEM_SPEC,
        scratch_shapes=[
            pltpu.VMEM(sizes + (seqs, width), BF16),
            pltpu.VMEM((chunks, plane, 8, 128), F32),
            pltpu.VMEM((8, 128), F32),
            pltpu.VMEM(block, BF16),
            pltpu.VMEM(block, BF16),
        ]
        + [pltpu.VMEM(w.shape, BF16) for w in weights]
        + [
            pltpu.VMEM((depth, width), BF16),
            pltpu.VMEM((depth, width), BF16),
            pltpu.VMEM((chunks, depth, width), BF16),
            pltpu.VMEM((chunks, plane * seqs, depth), BF16),
            pltpu.VMEM((chunks, slots, width), BF16),
            pltpu.VMEM((chunks * slots, weights[3].shape[2]), BF16),
            pltpu.VMEM((chunks, slots, 128), F32),
            pltpu.VMEM(sizes + block, BF16),
            [
                pltpu.VMEM((chunks, max(1, side - 1), side) + block, BF16),
                pltpu.VMEM((chunks, max(1, side - 1)) + block, BF16),
                pltpu.VMEM((max(1, chunks - 1),) + block, BF16),
            ],
            [
                dma((6,)),
                dma((2,)),
                dma((count,)),
                dma((count,)),
                hop,
                hop,
                hop,
                hop,
                dma((chunks,)),
                dma((chunks,)),
                hop,
                hop,
                dma((2,)),
            ],
        ],
        compiler_params=pltpu.CompilerParams(
            collective_id=0, has_side_effects=True, vmem_limit_bytes=VMEM_LIMIT
        ),
        name="layer_after",
    )(partial, hidden, gain, blend_vector, routing, route_scale, *weights)


def shards(
    hidden,
    mix_gain,
    recept_weight,
    key_weight,
    value_weight,
    decay_down,
    decay_up,
    decay_bias,
    rate_down,
    rate_up,
    rate_bias,
    head_gain,
    out_weight,
    memory_state,
    ffn_gain,
    blend_vector,
    dense_gate,
    dense_up,
    dense_down,
    expert_gate,
    expert_up,
    expert_down,
    routing,
    route_scale,
):
    sizes = factors_of(lax.axis_size("ep"))
    new_state, partial = attention(
        (
            hidden,
            mix_gain[None],
            decay_down.T,
            rate_down.T,
            decay_up,
            rate_up,
            decay_bias[None],
            rate_bias[None],
            recept_weight,
            key_weight,
            value_weight,
            head_gain[None],
            out_weight,
        ),
        memory_state,
    )
    layer_out = layer_after(
        sizes,
        partial,
        hidden,
        ffn_gain[None],
        blend_vector[None],
        routing.T,
        route_scale.T,
        (dense_gate.T, dense_up.T, dense_down, expert_gate, expert_up, expert_down),
    )
    return (layer_out, new_state)


def solution(mesh):
    in_specs = (
        P("ep", None),
        P(),
        P(None, "tp"),
        P(None, "tp"),
        P(None, "tp"),
        P(),
        P(),
        P(),
        P(),
        P(),
        P(),
        P(),
        P("tp", None),
        P("ep", "tp", None, None),
        P(),
        P(),
        P(None, ("ep", "tp")),
        P(None, ("ep", "tp")),
        P(("ep", "tp"), None),
        P("ep", None, "tp"),
        P("ep", None, "tp"),
        P("ep", "tp", None),
        P("ep", None),
        P("ep", None),
    )
    out_specs = (P("ep", None), P("ep", "tp", None, None))
    return jax.shard_map(shards, mesh=mesh, in_specs=in_specs, out_specs=out_specs, check_vma=False)
```

time: 124 us -> 96.4 us (0.78)
  matrix products: 25.8 us -> 0 us
  other arithmetic: 3.03 us -> 0 us
  Pallas kernels: 90.5 us -> 92.5 us
    dot_general x8 -> x0, matrix products: 25.8 us -> none  [the longest x7 22.4 us: matmul(): return jnp.dot(left, right, preferred_element_type=F32)]
    pallas_call x2 -> x1, Pallas kernels: 75.1 us -> 77.1 us  [layer_after(): pl.pallas_call(functools.partial(layer_kernel, sizes, top, cap), out_shap...]
    unnamed x14 -> x1, local copies, waits for them, and re-layouts: 2.99 us -> 1.67 us
    concatenate x1 -> x0, other arithmetic: 1.28 us -> none  [shards(): meta = jnp.concatenate([routing.T.astype(F32), route_scale.T], axis=0)]
where the time goes in v2:
time: 96.4 us; the launch traced here: 96.2 us
  Pallas kernels  92.5 us (96%)
  local copies, waits for them, and re-layouts  2.96 us (3%)
    pallas_call x1, Pallas kernels, layer_after(): pl.pallas_call(functools.partial(layer_kernel, sizes, top, cap), out_shap...  77.1 us
    pallas_call x1, Pallas kernels, attention(): pl.pallas_call(functools.partial(attention_kernel, chunks), out_shape=(ja...  15.5 us

profile of v2, /device:TPU:0, one launch (start us, length us, event | category | flops | bytes accessed | tf_op | source)
XLA Modules:
  0.0 96.2 jit_solution(11621274836756367428)
XLA Ops:
  0.6 1.3 %broadcast_in_dim.23.blend_vector = bf16[1,2048]{1,0:T(2,128)(2,1)} reshape(bf16[2048]{0:T(1024)(128)(2,1)} %param.39) | data formatting | bytes 8192 | tf_op jit(solution)/shard_map/broadcast_in_dim | solution.py:768
  1.9 15.5 %attention.1 = (f32[64,8,64,64]{3,2,1,0:T(8,128)}, bf16[64,2048]{1,0:T(8,128)(2,1)}) custom-call(bf16[64,2048]{1,0:T(8,128)(2,1)} %hidden.1, f32[1,2048]{1,0:T(1,128)} %bitcast.15, bf16[64,2048]{1,0:T(8,128)(2,1)} %bitcast.13, bf16[64,2048]{1,0:T(8,128)(2,1)} %bitcast.14, bf16[64,1024]{1,0:T(8,128)(2,1)} %refs_4_.1, bf16[64,1024]{1,0:T(8,128)(2,1)} %refs_5_.1, ...), custom_call_target="tpu_custom_call" | custom-call | tf_op jit(solution)/shard_map/attention/pallas_call | solution.py:174
  17.4 77.1 %layer_after.1 = bf16[64,2048]{1,0:T(8,128)(2,1)} custom-call(bf16[64,2048]{1,0:T(8,128)(2,1)} %get-tuple-element.4.partial, bf16[64,2048]{1,0:T(8,128)(2,1)} %hidden.1, f32[1,2048]{1,0:T(1,128)} %bitcast.16, bf16[1,2048]{1,0:T(2,128)(2,1)} %broadcast_in_dim.23.blend_vector, s32[2,64]{1,0:T(2,128)} %bitcast.20, f32[2,64]{1,0:T(2,128)} %bitcast.21, ...), custom_call_target="tpu_custom_call" | custom-call | tf_op jit(solution)/shard_map/layer_after/pallas_call | solution.py:668
  94.5 1.7 %copy.27 = bf16[64,2048]{1,0:T(8,128)(2,1)} copy(bf16[64,2048]{1,0:T(8,128)(2,1)} %layer_after.1) | data formatting | bytes 524288

commit v3 on v2

--- a/solution.py
+++ b/solution.py
@@ -249,6 +249,7 @@
     expert_down_h,
     out,
     tokens,
+    own_tokens,
     metas,
     meta,
     first,
@@ -264,8 +265,6 @@
     mix_w,
     mix_rows,
     picked,
-    expert_act,
-    slot_scale,
     from_sibling,
     lands,
     sems,
@@ -273,8 +272,7 @@
     (
         weight_sem,
         part_sem,
-        meta_send,
-        meta_recv,
+        meta_sem,
         ag_send,
         ag_recv,
         pass_send,
@@ -302,7 +300,7 @@
     blocks = across // rows_at_once
     block_chips = rows_at_once * along
     block_rows = block_chips * seqs
-    tile = 256
+    steps = max(sizes[1:]) - 1
 
     weights = (
         (gate_h, gate_v),
@@ -325,30 +323,22 @@
         def _():
             run(1)
 
+    def flat(stage, k, j):
+        return k if stage == 0 else chunks + ((stage - 1) * chunks + k) * steps + j - 1
+
     def meta_copy(k):
         peer = (ep + k) % count
-        place = metas.at[at[0], at[1] * along + at[2]]
-        return remote(meta, place, meta_send.at[k], meta_recv.at[k], (peer, tp))
-
-    for i in range(6):
-        weight_copy(i).start()
-    greet_all(count)
-    swap = remote(partial.at[other], sibling_part, part_sem.at[0], part_sem.at[1], sibling)
-    swap.start()
-    meta[...] = jnp.zeros(meta.shape, F32)
-    meta[0:top, 0:seqs] = routing[...].astype(F32)
-    meta[top : 2 * top, 0:seqs] = route_scale[...]
-    base = hidden[mine, :].astype(F32) + partial[mine, :].astype(F32)
-    swap.wait()
-    total = (base + sibling_part[...].astype(F32)).astype(BF16)
-    first[...] = total
-    tokens[at[0], at[1], at[2], mine, :] = rms_scaled(total.astype(F32), gain[...]).astype(BF16)
+        return remote(meta, metas.at[ep], meta_sem.at[0], meta_sem.at[1], (peer, tp))
 
     gather_orders = ((0, 2, 1), (0, 1, 2))
+    scatter_orders = ((1, 2), (2, 1))
+
+    def plane_of(k):
+        return (at[0] + chunks - k) % chunks
 
     def gather_view(core, stage, k, j):
         _, d2, d3 = gather_orders[core]
-        spot = [pl.ds((at[0] + chunks - k) % chunks, 1), None, None]
+        spot = [pl.ds(plane_of(k), 1), None, None]
 
         def one(d, back=0):
             return pl.ds((at[d] + sizes[d] - back) % sizes[d], 1)
@@ -359,95 +349,49 @@
 
     def gather_copy(core, stage, k, j):
         d = gather_orders[core][stage]
-        source = gather_view(core, stage, 0 if stage == 0 else k, 0)
+        target = gather_view(core, stage, 0 if stage == 0 else k, 0)
+        source = own_tokens if stage == 0 else target
         peer = ep + ((at[d] + j) % sizes[d] - at[d]) * strides[d]
-        slot = (stage, k, j if stage else 0)
-        return remote(source, source, ag_send.at[slot], ag_recv.at[slot], (peer, core))
-
-    def pass_copy(core, stage, k, j):
-        view, slot = gather_view(core, stage, k, j), (stage, k, j)
-        return remote(view, view, pass_send.at[slot], pass_recv.at[slot], sibling)
-
-    def pass_slots(core, k):
-        yield 0, k, 0
-        for stage in (1, 2):
-            for j in range(1, sizes[gather_orders[core][stage]]):
-                yield stage, k, j
-
-    def gather_begin(core):
+        slot = flat(stage, k, j)
+        return remote(source, target, ag_send.at[slot], ag_recv.at[slot], (peer, core))
+
+    def pass_on(core, stage, k, j):
+        view = gather_view(core, stage, k, j)
+        remote(view, view, pass_send.at[k], pass_recv.at[k], sibling).start()
+
+    def plane_pass(core, k):
+        view = tokens.at[plane_of(k), :, :, pl.ds(core * half, half)]
+        return remote(view, view, pass_send.at[k], pass_recv.at[k], sibling)
+
+    def send_first(core, k):
+        if k:
+            gather_copy(core, 0, k, k).wait()
         for j in range(1, sizes[gather_orders[core][1]]):
-            gather_copy(core, 1, 0, j).start()
-        for k in range(1, chunks):
-            gather_copy(core, 0, k, k).start()
-        pass_copy(core, 0, 0, 0).start()
-
-    def gather_step(core, t):
+            gather_copy(core, 1, k, j).start()
+        pass_on(core, 0, k, 0)
+
+    def send_second(core, k):
         order = gather_orders[core]
-
-        def later_phase(stage, k):
-            for j in range(1, sizes[order[stage]]):
-                gather_copy(core, stage, k, j).wait()
-            if stage == 1:
-                for j in range(1, sizes[order[2]]):
-                    gather_copy(core, 2, k, j).start()
-            for j in range(1, sizes[order[stage]]):
-                pass_copy(core, stage, k, j).start()
-
-        if 0 <= t - 1 < chunks:
-            later_phase(1, t - 1)
-        if 0 < t < chunks:
-            gather_copy(core, 0, t, t).wait()
-            for j in range(1, sizes[order[1]]):
-                gather_copy(core, 1, t, j).start()
-            pass_copy(core, 0, t, 0).start()
-        if 0 <= t - 2 < chunks:
-            later_phase(2, t - 2)
-
-    per_core(gather_begin)
-
-    def start_meta(k, carry):
-        meta_copy(k).start()
-        return carry
-
-    def wait_meta(k, carry):
-        meta_copy(k).wait()
-        return carry
-
-    lax.fori_loop(1, count, start_meta, 0)
-    metas[at[0], at[1] * along + at[2]] = meta[...]
-
-    for i in range(3):
-        weight_copy(i).wait()
-    top_row = lax.broadcasted_iota(jnp.int32, (slots, width), 0) == 0
-    gate_w[0:slots, :] = jnp.where(top_row, blend_vector[...].astype(F32), 0.0).astype(BF16)
-    up_w[0:slots, :] = jnp.zeros((slots, width), BF16)
-    if slots + units < depth:
-        rest = (depth - slots - units, width)
-        gate_w[slots + units : depth, :] = jnp.zeros(rest, BF16)
-        up_w[slots + units : depth, :] = jnp.zeros(rest, BF16)
-    gate_w[slots : slots + units, :] = gate_v[...]
-    up_w[slots : slots + units, :] = up_v[...]
-
-    def fill(z, carry):
-        if slots + units < depth:
-            mix_w[z, slots + units : depth, :] = jnp.zeros((depth - slots - units, width), BF16)
-        mix_w[z, slots : slots + units, :] = down_v[...]
-        return carry
-
-    lax.fori_loop(0, chunks, fill, 0)
-
-    def plane_of(k):
-        return (at[0] + chunks - k) % chunks
-
-    def use_tokens(k):
-        z = plane_of(k)
-
-        def arrive(core):
-            for slot in pass_slots(1 - core, k):
-                pass_copy(1 - core, *slot).wait_recv()
-
-        per_core(arrive)
-        here = metas[z]
+        for j in range(1, sizes[order[1]]):
+            gather_copy(core, 1, k, j).wait()
+        for j in range(1, sizes[order[2]]):
+            gather_copy(core, 2, k, j).start()
+        for j in range(1, sizes[order[1]]):
+            pass_on(core, 1, k, j)
+
+    def plane_done(core, k):
+        last = gather_orders[core][2]
+        for j in range(1, sizes[last]):
+            gather_copy(core, 2, k, j).wait()
+        for j in range(1, sizes[last]):
+            pass_on(core, 2, k, j)
+
+    def plane_here(core, k):
+        plane_pass(core, k).wait_send()
+        plane_pass(1 - core, k).wait_recv()
+
+    def select_of(k):
+        here = metas[pl.ds(plane_of(k) * plane, plane)]
         lanes = lax.broadcasted_iota(jnp.int32, (plane, 128), 1)
         expert = ep.astype(F32)
         chosen = jnp.zeros((plane, 128), F32)
@@ -461,7 +405,11 @@
         )
         rank = matmul(chosen.astype(BF16), jnp.where(earlier, 1.0, 0.0).astype(BF16))
         chip = lax.broadcasted_iota(jnp.int32, (plane, 128), 0).astype(F32)
-        place = jnp.where(chosen > 0.5, rank + chip * cap, -1.0)
+        return jnp.where(chosen > 0.5, rank + chip * cap, -1.0), scale_of
+
+    def use_tokens(k):
+        z = plane_of(k)
+        place, scale_of = select_of(k)
         scales = jnp.zeros((slots, 1), F32)
         for i in range(blocks):
             chips = range(i * block_chips, (i + 1) * block_chips)
@@ -470,20 +418,11 @@
             slot_of = lax.broadcasted_iota(jnp.int32, (depth, block_rows), 0).astype(F32)
             select = jnp.where(slot_of == place_row, 1.0, 0.0)
             scales = scales + jnp.sum(select[:slots] * scale_row, axis=1, keepdims=True)
-            ys = pl.ds(i * rows_at_once, rows_at_once)
             own_slots = slice(i * block_chips * cap, (i + 1) * block_chips * cap)
-            part = select[own_slots].astype(BF16)
-
-            def pick(n, carry):
-                cols = pl.ds(pl.multiple_of(n * tile, tile), tile)
-                found = matmul(part, tokens[z, ys, :, :, cols].reshape(block_rows, tile))
-                picked[z, own_slots, cols] = found.astype(BF16)
-                return carry
-
-            lax.fori_loop(0, width // tile, pick, 0)
             own_rows = slice(i * block_rows, (i + 1) * block_rows)
-            mix_rows[z, own_rows, :] = jnp.transpose(select).astype(BF16)
-        slot_scale[z] = jnp.broadcast_to(scales, (slots, 128))
+            rows = tokens[z, pl.ds(i * rows_at_once, rows_at_once)].reshape(block_rows, width)
+            picked[own_slots, :] = matmul(select[own_slots].astype(BF16), rows).astype(BF16)
+            mix_rows[own_rows, :] = jnp.transpose(select).astype(BF16)
 
         def dense(i, carry):
             rows = tokens[z, pl.ds(i * rows_at_once, rows_at_once)].reshape(block_rows, width)
@@ -491,55 +430,20 @@
             blend = 1.0 / (1.0 + jnp.exp(-gate[:, 0:1]))
             act = silu_of(gate) * matmul_nt(rows, up_w[...]) * blend
             own_rows = pl.ds(pl.multiple_of(i * block_rows, block_rows), block_rows)
-            mix_rows[z, own_rows, :] = (mix_rows[z, own_rows, :].astype(F32) + act).astype(BF16)
+            mix_rows[own_rows, :] = (mix_rows[own_rows, :].astype(F32) + act).astype(BF16)
             return carry
 
         lax.fori_loop(0, blocks, dense, 0)
-
-    for t in range(chunks + 2):
-        per_core(functools.partial(gather_step, t=t))
-        if t == 2:
-            lax.fori_loop(1, count, wait_meta, 0)
-        if t >= 3:
-            use_tokens(t - 3)
-    use_tokens(chunks - 1)
-
-    def passes_done(core):
-        for k in range(chunks):
-            for slot in pass_slots(core, k):
-                pass_copy(core, *slot).wait_send()
-
-    per_core(passes_done)
-
-    for i in range(3, 6):
-        weight_copy(i).wait()
-    slots_all = chunks * slots
-
-    def expert_hidden(n, carry):
-        cols = pl.ds(pl.multiple_of(n * tile, tile), tile)
-        rows = picked[...].reshape(slots_all, width)
-        gate = matmul(rows, expert_gate[0, :, cols])
-        expert_act[:, cols] = (silu_of(gate) * matmul(rows, expert_up[0, :, cols])).astype(BF16)
-        return carry
-
-    lax.fori_loop(0, expert_gate.shape[2] // tile, expert_hidden, 0)
-    scale_all = slot_scale[...].reshape(slots_all, 128)[:, 0:1]
-
-    def expert_result(n, carry):
-        cols = pl.ds(pl.multiple_of(n * tile, tile), tile)
-        result = (matmul(expert_act[...], expert_down[0, :, cols]) * scale_all).astype(BF16)
-        for z in range(chunks):
-            mix_w[z, 0:slots, cols] = result[z * slots : (z + 1) * slots]
-        return carry
-
-    lax.fori_loop(0, width // tile, expert_result, 0)
-
-    goals = [(at[0] + 1 + k) % chunks for k in range(chunks)]
-    scatter_orders = ((1, 2), (2, 1))
+        return scales
+
+    def run_experts(scales):
+        gate = matmul(picked[...], expert_gate[0])
+        hidden_rows = (silu_of(gate) * matmul(picked[...], expert_up[0])).astype(BF16)
+        mix_w[0:slots, :] = (matmul(hidden_rows, expert_down[0]) * scales).astype(BF16)
 
     def pair_copy(k):
         return remote(
-            tokens.at[goals[k], :, :, other],
+            tokens.at[plane_of(k), :, :, other],
             from_sibling.at[k],
             pair_send.at[k],
             pair_recv.at[k],
@@ -547,51 +451,50 @@
         )
 
     def make_part(k):
-        z = goals[k]
-
-        def some(n, carry):
-            cols = pl.ds(pl.multiple_of(n * tile, tile), tile)
-            for i in range(blocks):
-                own_rows = slice(i * block_rows, (i + 1) * block_rows)
-                part = matmul(mix_rows[z, own_rows, :], mix_w[z, :, cols]).astype(BF16)
-                ys = pl.ds(i * rows_at_once, rows_at_once)
-                tokens[z, ys, :, :, cols] = part.reshape(rows_at_once, along, seqs, tile)
+        z = plane_of(k)
+
+        def some(i, carry):
+            own_rows = pl.ds(pl.multiple_of(i * block_rows, block_rows), block_rows)
+            part = matmul(mix_rows[own_rows, :], mix_w[...]).astype(BF16)
+            ys = pl.ds(i * rows_at_once, rows_at_once)
+            tokens[z, ys] = part.reshape(rows_at_once, along, seqs, width)
             return carry
 
-        lax.fori_loop(0, width // tile, some, 0)
+        lax.fori_loop(0, blocks, some, 0)
         pair_copy(k).start()
 
     def spot(core, k, c1, c2):
         d1, d2 = scatter_orders[core]
-        place = [goals[k], None, None]
+        place = [plane_of(k), None, None]
         place[d1], place[d2] = c1, c2
         return tuple(place) + (pl.ds(core * half, half),)
 
     def scatter_copy(core, stage, k, j):
         d1, d2 = scatter_orders[core]
-        if stage == 0:
+        if stage == 1:
             d = d1
             source = tokens.at[spot(core, k, (at[d1] + j) % sizes[d1], slice(None))]
             target = lands[0].at[k, j - 1]
-        elif stage == 1:
+        elif stage == 2:
             d = d2
             source = tokens.at[spot(core, k, at[d1], (at[d2] + j) % sizes[d2])]
             target = lands[1].at[k, j - 1]
         else:
-            d = 0
+            d, j = 0, chunks - k
             source = tokens.at[spot(core, k, at[d1], at[d2])]
-            target = lands[2].at[k]
+            target = lands[2].at[k - 1]
         peer = ep + ((at[d] + j) % sizes[d] - at[d]) * strides[d]
-        slot = (stage, k, j if stage < 2 else 0)
+        slot = flat(stage, k, j)
         return remote(source, target, rs_send.at[slot], rs_recv.at[slot], (peer, core))
 
     def pair_sum(k):
         pair_copy(k).wait()
+        z = plane_of(k)
 
         def add(b, carry):
             y, x = b // along, b % along
-            tokens[goals[k], y, x, mine, :] = (
-                tokens[goals[k], y, x, mine, :].astype(F32) + from_sibling[k, y, x].astype(F32)
+            tokens[z, y, x, mine, :] = (
+                tokens[z, y, x, mine, :].astype(F32) + from_sibling[k, y, x].astype(F32)
             ).astype(BF16)
             return carry
 
@@ -599,14 +502,14 @@
 
         def send(core):
             for j in range(1, sizes[scatter_orders[core][0]]):
-                scatter_copy(core, 0, k, j).start()
+                scatter_copy(core, 1, k, j).start()
 
         per_core(send)
 
     def first_sum(core, k):
         d1, d2 = scatter_orders[core]
         for j in range(1, sizes[d1]):
-            scatter_copy(core, 0, k, j).wait()
+            scatter_copy(core, 1, k, j).wait()
 
         def add(b, carry):
             place = spot(core, k, at[d1], b)
@@ -618,35 +521,97 @@
 
         lax.fori_loop(0, sizes[d2], add, 0)
         for j in range(1, sizes[d2]):
-            scatter_copy(core, 1, k, j).start()
+            scatter_copy(core, 2, k, j).start()
 
     def second_sum(core, k):
         d1, d2 = scatter_orders[core]
         for j in range(1, sizes[d2]):
-            scatter_copy(core, 1, k, j).wait()
+            scatter_copy(core, 2, k, j).wait()
         place = spot(core, k, at[d1], at[d2])
         value = tokens[place].astype(F32)
         for j in range(1, sizes[d2]):
             value = value + lands[1][k, j - 1].astype(F32)
-        if k < chunks - 1:
-            tokens[place] = value.astype(BF16)
-            scatter_copy(core, 2, k, k + 1).start()
-            return
-        value = value + first[...].astype(F32)
-        for i in range(chunks - 1):
-            scatter_copy(core, 2, i, i + 1).wait()
-            value = value + lands[2][i].astype(F32)
+        tokens[place] = value.astype(BF16)
+        if k:
+            scatter_copy(core, 0, k, 0).start()
+
+    def finish(core):
+        value = tokens[spot(core, 0, at[scatter_orders[core][0]], at[scatter_orders[core][1]])]
+        value = value.astype(F32) + first[...].astype(F32)
+        for k in range(1, chunks):
+            scatter_copy(core, 0, k, 0).wait()
+            value = value + lands[2][k - 1].astype(F32)
         out[pl.ds(core * half, half), :] = value.astype(BF16)
 
-    for t in range(chunks + 3):
+    for i in range(6):
+        weight_copy(i).start()
+    meta[...] = jnp.zeros(meta.shape, F32)
+    meta[0:top, 0:seqs] = routing[...].astype(F32)
+    meta[top : 2 * top, 0:seqs] = route_scale[...]
+    base = hidden[mine, :].astype(F32) + partial[mine, :].astype(F32)
+    greet_all(count)
+    swap = remote(partial.at[other], sibling_part, part_sem.at[0], part_sem.at[1], sibling)
+    swap.start()
+
+    def start_meta(k, carry):
+        meta_copy(k).start()
+        return carry
+
+    lax.fori_loop(1, count, start_meta, 0)
+    swap.wait()
+    total = (base + sibling_part[...].astype(F32)).astype(BF16)
+    first[...] = total
+    normed = rms_scaled(total.astype(F32), gain[...]).astype(BF16)
+    own_tokens[0, 0, 0] = normed
+    tokens[at[0], at[1], at[2], mine, :] = normed
+
+    def start_planes(core):
+        send_first(core, 0)
+        for k in range(1, chunks):
+            gather_copy(core, 0, k, k).start()
+
+    per_core(start_planes)
+    metas[ep] = meta[...]
+    for i in range(3):
+        weight_copy(i).wait()
+    blend_row = jnp.concatenate(
+        [blend_vector[i : i + 1, :].astype(F32) for i in range(width // 128)], axis=1
+    )
+    top_row = lax.broadcasted_iota(jnp.int32, (slots, width), 0) == 0
+    gate_w[0:slots, :] = jnp.where(top_row, blend_row, 0.0).astype(BF16)
+    up_w[0:slots, :] = jnp.zeros((slots, width), BF16)
+    if slots + units < depth:
+        rest = (depth - slots - units, width)
+        gate_w[slots + units : depth, :] = jnp.zeros(rest, BF16)
+        up_w[slots + units : depth, :] = jnp.zeros(rest, BF16)
+        mix_w[slots + units : depth, :] = jnp.zeros(rest, BF16)
+    gate_w[slots : slots + units, :] = gate_v[...]
+    up_w[slots : slots + units, :] = up_v[...]
+    mix_w[slots : slots + units, :] = down_v[...]
+
+    def at_step(run, k):
+        if 0 <= k < chunks:
+            per_core(functools.partial(run, k=k))
+
+    for t in range(1, chunks + 4):
+        at_step(plane_done, t - 2)
+        if 0 <= t - 3 < chunks:
+            pair_sum(t - 3)
+        at_step(send_second, t - 1)
         if t < chunks:
-            make_part(t)
-        if 0 <= t - 1 < chunks:
-            pair_sum(t - 1)
+            at_step(send_first, t)
+        at_step(second_sum, t - 4)
         if 0 <= t - 2 < chunks:
-            per_core(functools.partial(first_sum, k=t - 2))
-        if 0 <= t - 3 < chunks:
-            per_core(functools.partial(second_sum, k=t - 3))
+            if t == 2:
+                some = metas.at[pl.ds(0, count - 1)]
+                remote(some, some, meta_sem.at[0], meta_sem.at[1], sibling).wait()
+                for i in range(3, 6):
+                    weight_copy(i).wait()
+            at_step(plane_here, t - 2)
+            run_experts(use_tokens(t - 2))
+            make_part(t - 2)
+        at_step(first_sum, t - 3)
+    per_core(finish)
 
     last = remote(out.at[mine], out.at[mine], last_sem.at[0], last_sem.at[1], sibling)
     last.start()
@@ -656,7 +621,7 @@
 def layer_after(sizes, partial, hidden, gain, blend_vector, routing, route_scale, weights):
     seqs, width = hidden.shape
     count = sizes[0] * sizes[1] * sizes[2]
-    half, top, most = seqs // 2, routing.shape[0], max(sizes)
+    half, top = seqs // 2, routing.shape[0]
     cap = max(2, 2 * seqs * top // count)
     plane = sizes[1] * sizes[2]
     slots = plane * cap
@@ -664,7 +629,7 @@
     chunks, side, block = sizes[0], max(sizes[1:]), (half, width)
     dma = pltpu.SemaphoreType.DMA
     any_spec = pl.BlockSpec(memory_space=pl.ANY)
-    hop = dma((3, chunks, most))
+    hop = dma((chunks * (2 * side - 1),))
     return pl.pallas_call(
         functools.partial(layer_kernel, sizes, top, cap),
         out_shape=jax.ShapeDtypeStruct((seqs, width), BF16),
@@ -672,7 +637,8 @@
         out_specs=VMEM_SPEC,
         scratch_shapes=[
             pltpu.VMEM(sizes + (seqs, width), BF16),
-            pltpu.VMEM((chunks, plane, 8, 128), F32),
+            pltpu.VMEM((1, 1, 1) + block, BF16),
+            pltpu.VMEM((count, 8, 128), F32),
             pltpu.VMEM((8, 128), F32),
             pltpu.VMEM(block, BF16),
             pltpu.VMEM(block, BF16),
@@ -681,11 +647,9 @@
         + [
             pltpu.VMEM((depth, width), BF16),
             pltpu.VMEM((depth, width), BF16),
-            pltpu.VMEM((chunks, depth, width), BF16),
-            pltpu.VMEM((chunks, plane * seqs, depth), BF16),
-            pltpu.VMEM((chunks, slots, width), BF16),
-            pltpu.VMEM((chunks * slots, weights[3].shape[2]), BF16),
-            pltpu.VMEM((chunks, slots, 128), F32),
+            pltpu.VMEM((depth, width), BF16),
+            pltpu.VMEM((plane * seqs, depth), BF16),
+            pltpu.VMEM((slots, width), BF16),
             pltpu.VMEM(sizes + block, BF16),
             [
                 pltpu.VMEM((chunks, max(1, side - 1), side) + block, BF16),
@@ -695,12 +659,11 @@
             [
                 dma((6,)),
                 dma((2,)),
-                dma((count,)),
-                dma((count,)),
+                dma((2,)),
                 hop,
                 hop,
-                hop,
-                hop,
+                dma((chunks,)),
+                dma((chunks,)),
                 dma((chunks,)),
                 dma((chunks,)),
                 hop,
@@ -765,7 +728,7 @@
         partial,
         hidden,
         ffn_gain[None],
-        blend_vector[None],
+        blend_vector.reshape(-1, 128),
         routing.T,
         route_scale.T,
         (dense_gate.T, dense_up.T, dense_down, expert_gate, expert_up, expert_down),

time: 96.4 us -> 88.7 us (0.920)
  Pallas kernels: 92.5 us -> 86.2 us
  local copies, waits for them, and re-layouts: 2.96 us -> 1.67 us
    pallas_call x1, Pallas kernels: 77.1 us -> 70.7 us  [layer_after(): pl.pallas_call(functools.partial(layer_kernel, sizes, top, cap), out_shap...]
    broadcast_in_dim x1 -> x0, local copies, waits for them, and re-layouts: 1.29 us -> none  [shards(): blend_vector[None]]
where the time goes in v3:
time: 88.7 us; the launch traced here: 88.5 us
  Pallas kernels  86.2 us (97%)
  local copies, waits for them, and re-layouts  1.67 us (2%)
    pallas_call x1, Pallas kernels, layer_after(): pl.pallas_call(functools.partial(layer_kernel, sizes, top, cap), out_shap...  70.7 us
    pallas_call x1, Pallas kernels, attention(): pl.pallas_call(functools.partial(attention_kernel, chunks), out_shape=(ja...  15.5 us

profile of v3, /device:TPU:0, one launch (start us, length us, event | category | flops | bytes accessed | tf_op | source)
XLA Modules:
  0.0 88.5 jit_solution(12803571383937324282)
XLA Ops:
  0.6 15.5 %attention.1 = (f32[64,8,64,64]{3,2,1,0:T(8,128)}, bf16[64,2048]{1,0:T(8,128)(2,1)}) custom-call(bf16[64,2048]{1,0:T(8,128)(2,1)} %hidden.1, f32[1,2048]{1,0:T(1,128)} %bitcast.16, bf16[64,2048]{1,0:T(8,128)(2,1)} %bitcast.14, bf16[64,2048]{1,0:T(8,128)(2,1)} %bitcast.15, bf16[64,1024]{1,0:T(8,128)(2,1)} %refs_4_.1, bf16[64,1024]{1,0:T(8,128)(2,1)} %refs_5_.1, ...), custom_call_target="tpu_custom_call" | custom-call | tf_op jit(solution)/shard_map/attention/pallas_call | solution.py:174
  16.1 70.7 %layer_after.1 = bf16[64,2048]{1,0:T(8,128)(2,1)} custom-call(bf16[64,2048]{1,0:T(8,128)(2,1)} %get-tuple-element.4.partial, bf16[64,2048]{1,0:T(8,128)(2,1)} %hidden.1, f32[1,2048]{1,0:T(1,128)} %bitcast.17, bf16[16,128]{1,0:T(8,128)(2,1)} %bitcast.21, s32[2,64]{1,0:T(2,128)} %bitcast.22, f32[2,64]{1,0:T(2,128)} %bitcast.23, bf16[176,2048]{1,0:T(8,128)(2,1)} %bitcast.12, ...), custom_call_target="tpu_custom_call" | custom-call | tf_op jit(solution)/shard_map/layer_after/pallas_call | solution.py:633
  86.9 1.7 %copy.27 = bf16[64,2048]{1,0:T(8,128)(2,1)} copy(bf16[64,2048]{1,0:T(8,128)(2,1)} %layer_after.1) | data formatting | bytes 524288

commit v4 on v3

--- a/solution.py
+++ b/solution.py
@@ -323,8 +323,11 @@
         def _():
             run(1)
 
-    def flat(stage, k, j):
-        return k if stage == 0 else chunks + ((stage - 1) * chunks + k) * steps + j - 1
+    def one_slot(k, j):
+        return chunks + k * steps + j - 1
+
+    def two_slot(k, j, i):
+        return chunks * (1 + steps) + (k * steps + j - 1) * (steps + 1) + i
 
     def meta_copy(k):
         peer = (ep + k) % count
@@ -336,27 +339,29 @@
     def plane_of(k):
         return (at[0] + chunks - k) % chunks
 
-    def gather_view(core, stage, k, j):
+    def gather_view(core, k, i, j):
         _, d2, d3 = gather_orders[core]
         spot = [pl.ds(plane_of(k), 1), None, None]
 
-        def one(d, back=0):
+        def one(d, back):
             return pl.ds((at[d] + sizes[d] - back) % sizes[d], 1)
 
-        spot[d2] = pl.ds(0, sizes[d2]) if stage == 2 else one(d2, j if stage == 1 else 0)
-        spot[d3] = one(d3, j if stage == 2 else 0)
+        spot[d2] = pl.ds(0, sizes[d2]) if i is None else one(d2, i)
+        spot[d3] = one(d3, j)
         return tokens.at[tuple(spot) + (pl.ds(core * half, half),)]
 
-    def gather_copy(core, stage, k, j):
-        d = gather_orders[core][stage]
-        target = gather_view(core, stage, 0 if stage == 0 else k, 0)
+    def peer_of(d, j):
+        return ep + ((at[d] + j) % sizes[d] - at[d]) * strides[d]
+
+    def gather_copy(core, stage, k, j, i=0):
+        target = gather_view(core, 0 if stage == 0 else k, i, 0)
         source = own_tokens if stage == 0 else target
-        peer = ep + ((at[d] + j) % sizes[d] - at[d]) * strides[d]
-        slot = flat(stage, k, j)
+        slot = (k, one_slot(k, j), two_slot(k, j, i))[stage]
+        peer = peer_of(gather_orders[core][stage], j)
         return remote(source, target, ag_send.at[slot], ag_recv.at[slot], (peer, core))
 
-    def pass_on(core, stage, k, j):
-        view = gather_view(core, stage, k, j)
+    def pass_on(core, k, i, j):
+        view = gather_view(core, k, i, j)
         remote(view, view, pass_send.at[k], pass_recv.at[k], sibling).start()
 
     def plane_pass(core, k):
@@ -364,27 +369,29 @@
         return remote(view, view, pass_send.at[k], pass_recv.at[k], sibling)
 
     def send_first(core, k):
+        order = gather_orders[core]
         if k:
             gather_copy(core, 0, k, k).wait()
-        for j in range(1, sizes[gather_orders[core][1]]):
+        for j in range(1, sizes[order[1]]):
             gather_copy(core, 1, k, j).start()
-        pass_on(core, 0, k, 0)
+        for j in range(1, sizes[order[2]]):
+            gather_copy(core, 2, k, j, 0).start()
+        pass_on(core, k, 0, 0)
 
     def send_second(core, k):
         order = gather_orders[core]
-        for j in range(1, sizes[order[1]]):
-            gather_copy(core, 1, k, j).wait()
+        for i in range(1, sizes[order[1]]):
+            gather_copy(core, 1, k, i).wait()
+            for j in range(1, sizes[order[2]]):
+                gather_copy(core, 2, k, j, i).start()
+            pass_on(core, k, i, 0)
+
+    def plane_done(core, k):
+        order = gather_orders[core]
         for j in range(1, sizes[order[2]]):
-            gather_copy(core, 2, k, j).start()
-        for j in range(1, sizes[order[1]]):
-            pass_on(core, 1, k, j)
-
-    def plane_done(core, k):
-        last = gather_orders[core][2]
-        for j in range(1, sizes[last]):
-            gather_copy(core, 2, k, j).wait()
-        for j in range(1, sizes[last]):
-            pass_on(core, 2, k, j)
+            for i in range(sizes[order[1]]):
+                gather_copy(core, 2, k, j, i).wait()
+            pass_on(core, k, None, j)
 
     def plane_here(core, k):
         plane_pass(core, k).wait_send()
@@ -422,7 +429,7 @@
             own_rows = slice(i * block_rows, (i + 1) * block_rows)
             rows = tokens[z, pl.ds(i * rows_at_once, rows_at_once)].reshape(block_rows, width)
             picked[own_slots, :] = matmul(select[own_slots].astype(BF16), rows).astype(BF16)
-            mix_rows[own_rows, :] = jnp.transpose(select).astype(BF16)
+            mix_rows[0, own_rows, :] = jnp.transpose(select).astype(BF16)
 
         def dense(i, carry):
             rows = tokens[z, pl.ds(i * rows_at_once, rows_at_once)].reshape(block_rows, width)
@@ -430,16 +437,17 @@
             blend = 1.0 / (1.0 + jnp.exp(-gate[:, 0:1]))
             act = silu_of(gate) * matmul_nt(rows, up_w[...]) * blend
             own_rows = pl.ds(pl.multiple_of(i * block_rows, block_rows), block_rows)
-            mix_rows[own_rows, :] = (mix_rows[own_rows, :].astype(F32) + act).astype(BF16)
+            routed = mix_rows[0, own_rows, :].astype(F32)
+            mix_rows[0, own_rows, :] = (routed + act).astype(BF16)
             return carry
 
         lax.fori_loop(0, blocks, dense, 0)
         return scales
 
-    def run_experts(scales):
+    def run_experts(k, scales):
         gate = matmul(picked[...], expert_gate[0])
         hidden_rows = (silu_of(gate) * matmul(picked[...], expert_up[0])).astype(BF16)
-        mix_w[0:slots, :] = (matmul(hidden_rows, expert_down[0]) * scales).astype(BF16)
+        mix_w[0, 0:slots, :] = (matmul(hidden_rows, expert_down[0]) * scales).astype(BF16)
 
     def pair_copy(k):
         return remote(
@@ -455,7 +463,7 @@
 
         def some(i, carry):
             own_rows = pl.ds(pl.multiple_of(i * block_rows, block_rows), block_rows)
-            part = matmul(mix_rows[own_rows, :], mix_w[...]).astype(BF16)
+            part = matmul(mix_rows[0, own_rows, :], mix_w[0]).astype(BF16)
             ys = pl.ds(i * rows_at_once, rows_at_once)
             tokens[z, ys] = part.reshape(rows_at_once, along, seqs, width)
             return carry
@@ -463,28 +471,21 @@
         lax.fori_loop(0, blocks, some, 0)
         pair_copy(k).start()
 
-    def spot(core, k, c1, c2):
+    def spot(core, k, j=0, i=0):
         d1, d2 = scatter_orders[core]
         place = [plane_of(k), None, None]
-        place[d1], place[d2] = c1, c2
+        place[d1], place[d2] = (at[d1] + j) % sizes[d1], (at[d2] + i) % sizes[d2]
         return tuple(place) + (pl.ds(core * half, half),)
 
-    def scatter_copy(core, stage, k, j):
+    def scatter_copy(core, stage, k, j=0, i=0):
         d1, d2 = scatter_orders[core]
-        if stage == 1:
-            d = d1
-            source = tokens.at[spot(core, k, (at[d1] + j) % sizes[d1], slice(None))]
-            target = lands[0].at[k, j - 1]
-        elif stage == 2:
-            d = d2
-            source = tokens.at[spot(core, k, at[d1], (at[d2] + j) % sizes[d2])]
-            target = lands[1].at[k, j - 1]
+        if stage == 0:
+            peer, slot, target = peer_of(0, chunks - k), k, lands[2].at[k - 1]
+        elif stage == 1:
+            peer, slot, target = peer_of(d1, j), two_slot(k, j, i), lands[0].at[k, j - 1, i]
         else:
-            d, j = 0, chunks - k
-            source = tokens.at[spot(core, k, at[d1], at[d2])]
-            target = lands[2].at[k - 1]
-        peer = ep + ((at[d] + j) % sizes[d] - at[d]) * strides[d]
-        slot = flat(stage, k, j)
+            peer, slot, target = peer_of(d2, i), one_slot(k, i), lands[1].at[k, i - 1]
+        source = tokens.at[spot(core, k, j, i)]
         return remote(source, target, rs_send.at[slot], rs_recv.at[slot], (peer, core))
 
     def pair_sum(k):
@@ -501,45 +502,42 @@
         lax.fori_loop(0, plane, add, 0)
 
         def send(core):
-            for j in range(1, sizes[scatter_orders[core][0]]):
-                scatter_copy(core, 1, k, j).start()
+            d1, d2 = scatter_orders[core]
+            for i in range(sizes[d2] - 1, -1, -1):
+                for j in range(1, sizes[d1]):
+                    scatter_copy(core, 1, k, j, i).start()
 
         per_core(send)
 
     def first_sum(core, k):
         d1, d2 = scatter_orders[core]
-        for j in range(1, sizes[d1]):
-            scatter_copy(core, 1, k, j).wait()
-
-        def add(b, carry):
-            place = spot(core, k, at[d1], b)
+        for i in range(sizes[d2] - 1, 0, -1):
+            place = spot(core, k, 0, i)
             value = tokens[place].astype(F32)
             for j in range(1, sizes[d1]):
-                value = value + lands[0][k, j - 1, b].astype(F32)
+                scatter_copy(core, 1, k, j, i).wait()
+                value = value + lands[0][k, j - 1, i].astype(F32)
             tokens[place] = value.astype(BF16)
-            return carry
-
-        lax.fori_loop(0, sizes[d2], add, 0)
-        for j in range(1, sizes[d2]):
-            scatter_copy(core, 2, k, j).start()
+            scatter_copy(core, 2, k, 0, i).start()
 
     def second_sum(core, k):
         d1, d2 = scatter_orders[core]
-        for j in range(1, sizes[d2]):
-            scatter_copy(core, 2, k, j).wait()
-        place = spot(core, k, at[d1], at[d2])
+        place = spot(core, k)
         value = tokens[place].astype(F32)
-        for j in range(1, sizes[d2]):
-            value = value + lands[1][k, j - 1].astype(F32)
+        for j in range(1, sizes[d1]):
+            scatter_copy(core, 1, k, j, 0).wait()
+            value = value + lands[0][k, j - 1, 0].astype(F32)
+        for i in range(1, sizes[d2]):
+            scatter_copy(core, 2, k, 0, i).wait()
+            value = value + lands[1][k, i - 1].astype(F32)
         tokens[place] = value.astype(BF16)
         if k:
-            scatter_copy(core, 0, k, 0).start()
+            scatter_copy(core, 0, k).start()
 
     def finish(core):
-        value = tokens[spot(core, 0, at[scatter_orders[core][0]], at[scatter_orders[core][1]])]
-        value = value.astype(F32) + first[...].astype(F32)
+        value = tokens[spot(core, 0)].astype(F32) + first[...].astype(F32)
         for k in range(1, chunks):
-            scatter_copy(core, 0, k, 0).wait()
+            scatter_copy(core, 0, k).wait()
             value = value + lands[2][k - 1].astype(F32)
         out[pl.ds(core * half, half), :] = value.astype(BF16)
 
@@ -584,33 +582,59 @@
         rest = (depth - slots - units, width)
         gate_w[slots + units : depth, :] = jnp.zeros(rest, BF16)
         up_w[slots + units : depth, :] = jnp.zeros(rest, BF16)
-        mix_w[slots + units : depth, :] = jnp.zeros(rest, BF16)
+        for b in range(2):
+            mix_w[b, slots + units : depth, :] = jnp.zeros(rest, BF16)
     gate_w[slots : slots + units, :] = gate_v[...]
     up_w[slots : slots + units, :] = up_v[...]
-    mix_w[slots : slots + units, :] = down_v[...]
-
-    def at_step(run, k):
+    for b in range(2):
+        mix_w[b, slots : slots + units, :] = down_v[...]
+
+    def on_core(run, k):
         if 0 <= k < chunks:
             per_core(functools.partial(run, k=k))
 
-    for t in range(1, chunks + 4):
-        at_step(plane_done, t - 2)
-        if 0 <= t - 3 < chunks:
-            pair_sum(t - 3)
-        at_step(send_second, t - 1)
-        if t < chunks:
-            at_step(send_first, t)
-        at_step(second_sum, t - 4)
-        if 0 <= t - 2 < chunks:
-            if t == 2:
-                some = metas.at[pl.ds(0, count - 1)]
-                remote(some, some, meta_sem.at[0], meta_sem.at[1], sibling).wait()
-                for i in range(3, 6):
-                    weight_copy(i).wait()
-            at_step(plane_here, t - 2)
-            run_experts(use_tokens(t - 2))
-            make_part(t - 2)
-        at_step(first_sum, t - 3)
+    def pair_step(k):
+        if 0 <= k < chunks:
+            pair_sum(k)
+
+    on_core(send_second, 0)
+    on_core(send_first, 1)
+    on_core(send_second, 1)
+    on_core(plane_done, 0)
+    on_core(send_first, 2)
+    some = metas.at[pl.ds(0, count - 1)]
+    remote(some, some, meta_sem.at[0], meta_sem.at[1], sibling).wait()
+    for i in range(3, 6):
+        weight_copy(i).wait()
+    on_core(plane_here, 0)
+    scales = use_tokens(0)
+    on_core(send_second, 2)
+    on_core(send_first, 3)
+    on_core(plane_done, 1)
+    run_experts(0, scales)
+    make_part(0)
+    for k in range(1, chunks):
+        on_core(plane_here, k)
+        scales = use_tokens(k)
+        on_core(send_second, k + 2)
+        on_core(send_first, k + 3)
+        pair_sum(k - 1)
+        if k > 2:
+            on_core(first_sum, k - 2)
+        run_experts(k, scales)
+        on_core(plane_done, k + 1)
+        make_part(k)
+        if k == 2:
+            on_core(first_sum, 0)
+    on_core(first_sum, chunks - 2) if chunks > 2 else None
+    pair_sum(chunks - 1)
+    if chunks == 2:
+        on_core(first_sum, 0)
+    on_core(second_sum, chunks - 4)
+    on_core(second_sum, chunks - 3)
+    on_core(second_sum, chunks - 2)
+    on_core(first_sum, chunks - 1)
+    on_core(second_sum, chunks - 1)
     per_core(finish)
 
     last = remote(out.at[mine], out.at[mine], last_sem.at[0], last_sem.at[1], sibling)
@@ -629,7 +653,7 @@
     chunks, side, block = sizes[0], max(sizes[1:]), (half, width)
     dma = pltpu.SemaphoreType.DMA
     any_spec = pl.BlockSpec(memory_space=pl.ANY)
-    hop = dma((chunks * (2 * side - 1),))
+    hop = dma((chunks * (side * side),))
     return pl.pallas_call(
         functools.partial(layer_kernel, sizes, top, cap),
         out_shape=jax.ShapeDtypeStruct((seqs, width), BF16),
@@ -647,8 +671,8 @@
         + [
             pltpu.VMEM((depth, width), BF16),
             pltpu.VMEM((depth, width), BF16),
-            pltpu.VMEM((depth, width), BF16),
-            pltpu.VMEM((plane * seqs, depth), BF16),
+            pltpu.VMEM((2, depth, width), BF16),
+            pltpu.VMEM((2, plane * seqs, depth), BF16),
             pltpu.VMEM((slots, width), BF16),
             pltpu.VMEM(sizes + block, BF16),
             [

time: 88.7 us -> 81.4 us (0.918)
  Pallas kernels: 86.2 us -> 78.9 us
    pallas_call x1, Pallas kernels: 70.7 us -> 63.4 us  [layer_after(): pl.pallas_call(functools.partial(layer_kernel, sizes, top, cap), out_shap...]
where the time goes in v4:
time: 81.4 us; the launch traced here: 81.2 us
  Pallas kernels  78.9 us (97%)
  local copies, waits for them, and re-layouts  1.67 us (2%)
    pallas_call x1, Pallas kernels, layer_after(): pl.pallas_call(functools.partial(layer_kernel, sizes, top, cap), out_shap...  63.4 us
    pallas_call x1, Pallas kernels, attention(): pl.pallas_call(functools.partial(attention_kernel, chunks), out_shape=(ja...  15.5 us
    unnamed x1, local copies, waits for them, and re-layouts  1.67 us

profile of v4, /device:TPU:0, one launch (start us, length us, event | category | flops | bytes accessed | tf_op | source)
XLA Modules:
  0.0 81.2 jit_solution(12296641174173346620)
XLA Ops:
  0.6 15.5 %attention.1 = (f32[64,8,64,64]{3,2,1,0:T(8,128)}, bf16[64,2048]{1,0:T(8,128)(2,1)}) custom-call(bf16[64,2048]{1,0:T(8,128)(2,1)} %hidden.1, f32[1,2048]{1,0:T(1,128)} %bitcast.16, bf16[64,2048]{1,0:T(8,128)(2,1)} %bitcast.14, bf16[64,2048]{1,0:T(8,128)(2,1)} %bitcast.15, bf16[64,1024]{1,0:T(8,128)(2,1)} %refs_4_.1, bf16[64,1024]{1,0:T(8,128)(2,1)} %refs_5_.1, ...), custom_call_target="tpu_custom_call" | custom-call | tf_op jit(solution)/shard_map/attention/pallas_call | solution.py:174
  16.1 63.4 %layer_after.1 = bf16[64,2048]{1,0:T(8,128)(2,1)} custom-call(bf16[64,2048]{1,0:T(8,128)(2,1)} %get-tuple-element.4.partial, bf16[64,2048]{1,0:T(8,128)(2,1)} %hidden.1, f32[1,2048]{1,0:T(1,128)} %bitcast.17, bf16[16,128]{1,0:T(8,128)(2,1)} %bitcast.21, s32[2,64]{1,0:T(2,128)} %bitcast.22, f32[2,64]{1,0:T(2,128)} %bitcast.23, bf16[176,2048]{1,0:T(8,128)(2,1)} %bitcast.12, ...), custom_call_target="tpu_custom_call" | custom-call | tf_op jit(solution)/shard_map/layer_after/pallas_call | solution.py:657
  79.5 1.7 %copy.27 = bf16[64,2048]{1,0:T(8,128)(2,1)} copy(bf16[64,2048]{1,0:T(8,128)(2,1)} %layer_after.1) | data formatting | bytes 524288

commit v5 on v4

--- a/solution.py
+++ b/solution.py
@@ -323,6 +323,11 @@
         def _():
             run(1)
 
+    order_of_planes = [0] + sorted(range(1, chunks), key=lambda k: (-min(k, chunks - k), k))
+
+    def buffer_of(k):
+        return order_of_planes.index(k) % 2
+
     def one_slot(k, j):
         return chunks + k * steps + j - 1
 
@@ -428,8 +433,8 @@
             own_slots = slice(i * block_chips * cap, (i + 1) * block_chips * cap)
             own_rows = slice(i * block_rows, (i + 1) * block_rows)
             rows = tokens[z, pl.ds(i * rows_at_once, rows_at_once)].reshape(block_rows, width)
-            picked[own_slots, :] = matmul(select[own_slots].astype(BF16), rows).astype(BF16)
-            mix_rows[0, own_rows, :] = jnp.transpose(select).astype(BF16)
+            picked[buffer_of(k), own_slots, :] = matmul(select[own_slots].astype(BF16), rows).astype(BF16)
+            mix_rows[buffer_of(k), own_rows, :] = jnp.transpose(select).astype(BF16)
 
         def dense(i, carry):
             rows = tokens[z, pl.ds(i * rows_at_once, rows_at_once)].reshape(block_rows, width)
@@ -437,17 +442,26 @@
             blend = 1.0 / (1.0 + jnp.exp(-gate[:, 0:1]))
             act = silu_of(gate) * matmul_nt(rows, up_w[...]) * blend
             own_rows = pl.ds(pl.multiple_of(i * block_rows, block_rows), block_rows)
-            routed = mix_rows[0, own_rows, :].astype(F32)
-            mix_rows[0, own_rows, :] = (routed + act).astype(BF16)
+            routed = mix_rows[buffer_of(k), own_rows, :].astype(F32)
+            mix_rows[buffer_of(k), own_rows, :] = (routed + act).astype(BF16)
             return carry
 
         lax.fori_loop(0, blocks, dense, 0)
         return scales
 
-    def run_experts(k, scales):
-        gate = matmul(picked[...], expert_gate[0])
-        hidden_rows = (silu_of(gate) * matmul(picked[...], expert_up[0])).astype(BF16)
-        mix_w[0, 0:slots, :] = (matmul(hidden_rows, expert_down[0]) * scales).astype(BF16)
+    def run_experts(ks, scales):
+        if len(ks) == 2:
+            rows = picked[...].reshape(2 * slots, width)
+            scales = jnp.concatenate(scales if buffer_of(ks[0]) == 0 else scales[::-1], axis=0)
+        else:
+            rows, scales = picked[buffer_of(ks[0])], scales[0]
+        gate = matmul(rows, expert_gate[0])
+        hidden_rows = (silu_of(gate) * matmul(rows, expert_up[0])).astype(BF16)
+        result = (matmul(hidden_rows, expert_down[0]) * scales).astype(BF16)
+        if len(ks) == 2:
+            mix_w[:, 0:slots, :] = result.reshape(2, slots, width)
+        else:
+            mix_w[buffer_of(ks[0]), 0:slots, :] = result
 
     def pair_copy(k):
         return remote(
@@ -463,7 +477,7 @@
 
         def some(i, carry):
             own_rows = pl.ds(pl.multiple_of(i * block_rows, block_rows), block_rows)
-            part = matmul(mix_rows[0, own_rows, :], mix_w[0]).astype(BF16)
+            part = matmul(mix_rows[buffer_of(k), own_rows, :], mix_w[buffer_of(k)]).astype(BF16)
             ys = pl.ds(i * rows_at_once, rows_at_once)
             tokens[z, ys] = part.reshape(rows_at_once, along, seqs, width)
             return carry
@@ -503,11 +517,15 @@
 
         def send(core):
             d1, d2 = scatter_orders[core]
-            for i in range(sizes[d2] - 1, -1, -1):
+            for i in range(sizes[d2] - 1, 0, -1):
                 for j in range(1, sizes[d1]):
                     scatter_copy(core, 1, k, j, i).start()
 
         per_core(send)
+
+    def send_kept(core, k):
+        for j in range(1, sizes[scatter_orders[core][0]]):
+            scatter_copy(core, 1, k, j, 0).start()
 
     def first_sum(core, k):
         d1, d2 = scatter_orders[core]
@@ -565,7 +583,7 @@
 
     def start_planes(core):
         send_first(core, 0)
-        for k in range(1, chunks):
+        for k in order_of_planes[1:]:
             gather_copy(core, 0, k, k).start()
 
     per_core(start_planes)
@@ -591,12 +609,14 @@
 
     def on_core(run, k):
         if 0 <= k < chunks:
-            per_core(functools.partial(run, k=k))
+            per_core(functools.partial(run, k=order_of_planes[k]))
 
     def pair_step(k):
         if 0 <= k < chunks:
-            pair_sum(k)
-
+            pair_sum(order_of_planes[k])
+            on_core(send_kept, k)
+
+    joint = [k for k in (chunks - 2, chunks - 1) if k > 0]
     on_core(send_second, 0)
     on_core(send_first, 1)
     on_core(send_second, 1)
@@ -607,34 +627,45 @@
     for i in range(3, 6):
         weight_copy(i).wait()
     on_core(plane_here, 0)
-    scales = use_tokens(0)
+    scales = [use_tokens(0)]
     on_core(send_second, 2)
     on_core(send_first, 3)
     on_core(plane_done, 1)
-    run_experts(0, scales)
+    run_experts([0], scales)
     make_part(0)
-    for k in range(1, chunks):
+    for k in range(1, chunks - 2):
         on_core(plane_here, k)
-        scales = use_tokens(k)
+        scales = [use_tokens(order_of_planes[k])]
         on_core(send_second, k + 2)
         on_core(send_first, k + 3)
-        pair_sum(k - 1)
-        if k > 2:
+        pair_step(k - 1)
+        on_core(first_sum, k - 2)
+        run_experts([order_of_planes[k]], scales)
+        on_core(plane_done, k + 1)
+        make_part(order_of_planes[k])
+    scales = []
+    for k in joint:
+        on_core(plane_here, k)
+        scales.append(use_tokens(order_of_planes[k]))
+        if k == joint[0]:
+            pair_step(k - 1)
+            on_core(plane_done, k + 1)
             on_core(first_sum, k - 2)
-        run_experts(k, scales)
-        on_core(plane_done, k + 1)
-        make_part(k)
-        if k == 2:
-            on_core(first_sum, 0)
-    on_core(first_sum, chunks - 2) if chunks > 2 else None
-    pair_sum(chunks - 1)
-    if chunks == 2:
-        on_core(first_sum, 0)
+    if joint:
+        run_experts([order_of_planes[k] for k in joint], scales)
+    for k in joint:
+        make_part(order_of_planes[k])
+    on_core(first_sum, chunks - 3)
+    for k in joint or [0]:
+        pair_sum(order_of_planes[k])
+    for k in joint or [0]:
+        on_core(send_kept, k)
     on_core(second_sum, chunks - 4)
     on_core(second_sum, chunks - 3)
-    on_core(second_sum, chunks - 2)
-    on_core(first_sum, chunks - 1)
-    on_core(second_sum, chunks - 1)
+    for k in joint or [0]:
+        on_core(first_sum, k)
+    for k in joint or [0]:
+        on_core(second_sum, k)
     per_core(finish)
 
     last = remote(out.at[mine], out.at[mine], last_sem.at[0], last_sem.at[1], sibling)
@@ -673,7 +704,7 @@
             pltpu.VMEM((depth, width), BF16),
             pltpu.VMEM((2, depth, width), BF16),
             pltpu.VMEM((2, plane * seqs, depth), BF16),
-            pltpu.VMEM((slots, width), BF16),
+            pltpu.VMEM((2, slots, width), BF16),
             pltpu.VMEM(sizes + block, BF16),
             [
                 pltpu.VMEM((chunks, max(1, side - 1), side) + block, BF16),

time: 81.4 us -> 80.1 us (0.984)
  Pallas kernels: 78.9 us -> 77.6 us
    pallas_call x1, Pallas kernels: 63.4 us -> 62.1 us  [layer_after(): pl.pallas_call(functools.partial(layer_kernel, sizes, top, cap), out_shap...]
where the time goes in v5:
time: 80.1 us; the launch traced here: 79.9 us
  Pallas kernels  77.6 us (97%)
  local copies, waits for them, and re-layouts  1.67 us (2%)
    pallas_call x1, Pallas kernels, layer_after(): pl.pallas_call(functools.partial(layer_kernel, sizes, top, cap), out_shap...  62.1 us
    pallas_call x1, Pallas kernels, attention(): pl.pallas_call(functools.partial(attention_kernel, chunks), out_shape=(ja...  15.5 us
    unnamed x1, local copies, waits for them, and re-layouts  1.67 us

profile of v5, /device:TPU:0, one launch (start us, length us, event | category | flops | bytes accessed | tf_op | source)
XLA Modules:
  0.0 79.9 jit_solution(9899416512356977695)
XLA Ops:
  0.6 15.5 %attention.1 = (f32[64,8,64,64]{3,2,1,0:T(8,128)}, bf16[64,2048]{1,0:T(8,128)(2,1)}) custom-call(bf16[64,2048]{1,0:T(8,128)(2,1)} %hidden.1, f32[1,2048]{1,0:T(1,128)} %bitcast.16, bf16[64,2048]{1,0:T(8,128)(2,1)} %bitcast.14, bf16[64,2048]{1,0:T(8,128)(2,1)} %bitcast.15, bf16[64,1024]{1,0:T(8,128)(2,1)} %refs_4_.1, bf16[64,1024]{1,0:T(8,128)(2,1)} %refs_5_.1, ...), custom_call_target="tpu_custom_call" | custom-call | tf_op jit(solution)/shard_map/attention/pallas_call | solution.py:174
  16.1 62.1 %layer_after.1 = bf16[64,2048]{1,0:T(8,128)(2,1)} custom-call(bf16[64,2048]{1,0:T(8,128)(2,1)} %get-tuple-element.4.partial, bf16[64,2048]{1,0:T(8,128)(2,1)} %hidden.1, f32[1,2048]{1,0:T(1,128)} %bitcast.17, bf16[16,128]{1,0:T(8,128)(2,1)} %bitcast.21, s32[2,64]{1,0:T(2,128)} %bitcast.22, f32[2,64]{1,0:T(2,128)} %bitcast.23, bf16[176,2048]{1,0:T(8,128)(2,1)} %bitcast.12, ...), custom_call_target="tpu_custom_call" | custom-call | tf_op jit(solution)/shard_map/layer_after/pallas_call | solution.py:688
  78.3 1.7 %copy.27 = bf16[64,2048]{1,0:T(8,128)(2,1)} copy(bf16[64,2048]{1,0:T(8,128)(2,1)} %layer_after.1) | data formatting | bytes 524288

commit v6 on v5

--- a/solution.py
+++ b/solution.py
@@ -167,7 +167,7 @@
     seqs, heads, size, _ = state.shape
     hidden = operands[0]
     width = heads * size
-    chunks = seqs // math.gcd(seqs, 8)
+    chunks = seqs // math.gcd(seqs, 4)
     per_head = pltpu.VMEM((heads, seqs, size), F32)
     dma = pltpu.SemaphoreType.DMA
     any_spec = pl.BlockSpec(memory_space=pl.ANY)
@@ -657,9 +657,7 @@
         make_part(order_of_planes[k])
     on_core(first_sum, chunks - 3)
     for k in joint or [0]:
-        pair_sum(order_of_planes[k])
-    for k in joint or [0]:
-        on_core(send_kept, k)
+        pair_step(k)
     on_core(second_sum, chunks - 4)
     on_core(second_sum, chunks - 3)
     for k in joint or [0]:

time: 80.1 us -> 80.3 us (level)
  no operation moved by 1% of the time
where the time goes in v6:
time: 80.3 us; the launch traced here: 80.1 us
  Pallas kernels  77.8 us (97%)
  local copies, waits for them, and re-layouts  1.67 us (2%)
    pallas_call x1, Pallas kernels, layer_after(): pl.pallas_call(functools.partial(layer_kernel, sizes, top, cap), out_shap...  62.1 us
    pallas_call x1, Pallas kernels, attention(): pl.pallas_call(functools.partial(attention_kernel, chunks), out_shape=(ja...  15.7 us
    unnamed x1, local copies, waits for them, and re-layouts  1.67 us

profile of v6, /device:TPU:0, one launch (start us, length us, event | category | flops | bytes accessed | tf_op | source)
XLA Modules:
  0.0 80.1 jit_solution(18040788352154187872)
XLA Ops:
  0.6 15.7 %attention.1 = (f32[64,8,64,64]{3,2,1,0:T(8,128)}, bf16[64,2048]{1,0:T(8,128)(2,1)}) custom-call(bf16[64,2048]{1,0:T(8,128)(2,1)} %hidden.1, f32[1,2048]{1,0:T(1,128)} %bitcast.16, bf16[64,2048]{1,0:T(8,128)(2,1)} %bitcast.14, bf16[64,2048]{1,0:T(8,128)(2,1)} %bitcast.15, bf16[64,1024]{1,0:T(8,128)(2,1)} %refs_4_.1, bf16[64,1024]{1,0:T(8,128)(2,1)} %refs_5_.1, ...), custom_call_target="tpu_custom_call" | custom-call | tf_op jit(solution)/shard_map/attention/pallas_call | solution.py:174
  16.3 62.1 %layer_after.1 = bf16[64,2048]{1,0:T(8,128)(2,1)} custom-call(bf16[64,2048]{1,0:T(8,128)(2,1)} %get-tuple-element.4.partial, bf16[64,2048]{1,0:T(8,128)(2,1)} %hidden.1, f32[1,2048]{1,0:T(1,128)} %bitcast.17, bf16[16,128]{1,0:T(8,128)(2,1)} %bitcast.21, s32[2,64]{1,0:T(2,128)} %bitcast.22, f32[2,64]{1,0:T(2,128)} %bitcast.23, bf16[176,2048]{1,0:T(8,128)(2,1)} %bitcast.12, ...), custom_call_target="tpu_custom_call" | custom-call | tf_op jit(solution)/shard_map/layer_after/pallas_call | solution.py:686
  78.4 1.7 %copy.27 = bf16[64,2048]{1,0:T(8,128)(2,1)} copy(bf16[64,2048]{1,0:T(8,128)(2,1)} %layer_after.1) | data formatting | bytes 524288
